TPU v7x, 512 devices: a 8x2x16 block of a 8x16x16 slice. The times are simulated.
512 devices in a mesh: grp: 2 (over y), ep: 16 (over z), tp: 16 (over x, core).
Axes of the slice: x: 8, y: 2, z: 16, core: 2. Of those that a mesh axis runs over, the one named last changes fastest.
The devices are a block of a 8x16x16 slice.
Arguments:
- mix_query: bfloat16 [16384, 16, 128], P(('grp', 'ep'), 'tp'), parts along dimension 0, may hold values from -6 to 6
- mix_keys: bfloat16 [16384, 16, 128], P(('grp', 'ep'), 'tp'), parts along dimension 0, may hold values from -6 to 6
- mix_values: bfloat16 [16384, 16, 128], P(('grp', 'ep'), 'tp'), parts along dimension 0, may hold values from -6 to 6
- beta_in: float32 [16, 16384], P('tp', ('grp', 'ep')), parts along dimension 1, may hold values from -9.5 to 6
- decay_in: float32 [16, 16384], P('tp', ('grp', 'ep')), parts along dimension 1, may hold values from -14 to 0
- norm_gain: float32 [128], replicated, may hold values from 0.1 to 1.9
- ffn_input: bfloat16 [4096, 4096], P(('grp', 'ep'), 'tp'), parts along dimension 0, may hold values from -200 to 200
- ffn_gain: float32 [4096], P('tp'), may hold values from 0.1 to 1.9
- expert_ids: int32 [4096, 2], P(('grp', 'ep')), parts along dimension 0, may hold values from 0 to 15, as said below
- expert_share: float32 [4096, 2], P(('grp', 'ep')), parts along dimension 0, may hold values from 0.2 to 1
- w_gate: bfloat16 [16, 4096, 1024], P('ep', None, 'tp'), may hold values from -0.09375 to 0.09375
- w_up: bfloat16 [16, 4096, 1024], P('ep', None, 'tp'), may hold values from -0.09375 to 0.09375
- w_down: bfloat16 [16, 1024, 4096], P('ep', None, 'tp'), may hold values from -0.1875 to 0.1875
Outputs:
- mix_out: bfloat16 [16384, 16, 128], P(('grp', 'ep'), 'tp'), parts along dimension 0
- ffn_out: bfloat16 [4096, 4096], P(('grp', 'ep'), 'tp'), parts along dimension 0
There are 2 independent parts, one for each index of `grp`. A program takes and returns all parts, laid end to end along the dimension named above; an argument that names none is the same for every part. Nothing has to cross between parts.
Inputs may be any that keep to these rules, and one draw needn't show every extreme that they name: `expert_ids`: each row names two different experts of one group, the group being id // 4; the rows of one device (aligned blocks of 128 rows) name every expert exactly 2 * 128 // 16 times.
All inputs are finite; a program needn't handle non-finite values.
Results may differ from a plain program's by a relative error of at most 0.007.
Values may be sent and summed in bfloat16 or wider, within the bound.
A program may use at most 64 MiB of HBM per device.

v0:
```python
import jax
import jax.numpy as jnp
from jax import lax
from jax.sharding import Mesh
from jax.sharding import PartitionSpec as P

BLOCK = 64
TP = ("tp_0", "tp_1")


PRECISE = lax.Precision.HIGHEST
EPSILON = 1e-06


def sent_together(arrays, axis, dim, along):
    widths = [a.shape[along] for a in arrays]
    both = jnp.concatenate(arrays, axis=along)
    result = lax.all_gather(both, axis, axis=dim, tiled=True)
    return tuple(jnp.split(result, [sum(widths[:k]) for k in range(1, len(widths))], axis=along))


def from_everyone(x, axis):
    size = lax.axis_size(axis)
    return lax.all_to_all(jnp.broadcast_to(x[None], (size, *x.shape)), axis, 0, 0, tiled=True)


def of_everyone(x, axis):
    return from_everyone(x, axis).sum(axis=0)


def joined_along(pieces, dim):
    pieces = jnp.moveaxis(pieces, 0, dim)
    shape = pieces.shape
    return pieces.reshape(*shape[:dim], shape[dim] * shape[dim + 1], *shape[dim + 2 :])


def gather_directly(x, axis, dim):
    pieces = from_everyone(x, axis)
    return joined_along(pieces, dim)


def gather_axes(x, axes, dim):
    result = x
    for number in range(len(axes) - 1, -1, -1):
        result = lax.all_gather(result, axes[number], axis=dim, tiled=True)
    return result


def unit_inverse(strict_lower):
    extent = strict_lower.shape[-1]
    identity = jnp.eye(extent, dtype=jnp.float32)
    powered = -strict_lower
    product = identity + powered
    for section_index in range(1, (extent - 1).bit_length()):
        powered = jnp.matmul(powered, powered, precision=PRECISE)
        product = jnp.matmul(product, identity + powered, precision=PRECISE)
    return product


def block_terms(queries, keyset, valueset, betas, rates):
    extent = queries.shape[-2]
    cumulative = -jnp.cumsum(rates, axis=-1)
    positions = jnp.arange(extent)
    causal = positions[:, None] >= positions[None, :]
    strict = positions[:, None] > positions[None, :]
    spread = cumulative[..., :, None] - cumulative[..., None, :]
    decay_mask = jnp.where(causal, jnp.exp(jnp.where(causal, spread, 0.0)), 0.0)
    keys_beta = keyset * betas[..., None]
    values_beta = valueset * betas[..., None]
    lower_part = jnp.where(
        strict,
        jnp.einsum("...id,...jd->...ij", keys_beta, keyset, precision=PRECISE) * decay_mask,
        0.0,
    )
    inverse = unit_inverse(lower_part)
    update = jnp.einsum("...ij,...jd->...id", inverse, values_beta, precision=PRECISE)
    correction = jnp.einsum(
        "...ij,...jd->...id", inverse, keys_beta * jnp.exp(cumulative)[..., None], precision=PRECISE
    )
    scores = jnp.where(
        causal,
        jnp.einsum("...id,...jd->...ij", queries, keyset, precision=PRECISE) * decay_mask,
        0.0,
    )
    query_decay = queries * jnp.exp(cumulative)[..., None]
    key_decay = keyset * jnp.exp(cumulative[..., -1:] - cumulative)[..., None]
    block_decay = jnp.exp(cumulative[..., -1])
    return (query_decay, key_decay, update, correction, scores, block_decay)


def unit_rows(values_in, factor):
    floats = values_in.astype(jnp.float32)
    return floats * lax.rsqrt(jnp.sum(floats * floats, -1, keepdims=True) + EPSILON) * factor


def compose(earlier, later):
    return (
        jnp.matmul(later[0], earlier[0], precision=PRECISE),
        jnp.matmul(later[0], earlier[1], precision=PRECISE) + later[1],
    )


def mixer_body(mix_query, mix_keys, mix_values, beta_in, decay_in, norm_gain):
    length, head_count, width = mix_query.shape
    blocks = length // BLOCK

    def to_blocks(tensor):
        return tensor.reshape(blocks, BLOCK, head_count, width).transpose(2, 0, 1, 3)

    queries = to_blocks(unit_rows(mix_query, width ** (-0.5)))
    keyset = to_blocks(unit_rows(mix_keys, 1.0))
    valueset = to_blocks(mix_values.astype(jnp.float32))
    betas = jax.nn.sigmoid(beta_in).reshape(head_count, blocks, BLOCK)
    rates = jax.nn.softplus(decay_in).reshape(head_count, blocks, BLOCK)
    query_decay, key_decay, update, correction, scores, block_decay = block_terms(
        queries, keyset, valueset, betas, rates
    )
    identity = jnp.eye(width, dtype=jnp.float32)
    transfer = block_decay[..., None, None] * identity - jnp.einsum(
        "hncd,hnce->hnde", key_decay, correction, precision=PRECISE
    )
    offset = jnp.einsum("hncd,hnce->hnde", key_decay, update, precision=PRECISE)
    prefix_map, prefix_add = lax.associative_scan(compose, (transfer, offset), axis=1)
    total_map = prefix_map[:, -1]
    total_add = prefix_add[:, -1]
    empty_state = jnp.zeros((head_count, width, width), jnp.float32)
    all_maps, all_adds = sent_together((total_map[None], total_add[None]), "ep", 0, 1)
    position = lax.axis_index("ep")

    def absorb(member, carried):
        advanced = jnp.matmul(all_maps[member], carried, precision=PRECISE) + all_adds[member]
        return jnp.where(member < position, advanced, carried)

    entering = lax.fori_loop(0, lax.axis_size("ep"), absorb, empty_state)
    after_blocks = jnp.matmul(prefix_map, entering[:, None], precision=PRECISE) + prefix_add
    starts = jnp.concatenate([entering[:, None], after_blocks[:, :-1]], axis=1)
    fresh = update - jnp.einsum("hncd,hnde->hnce", correction, starts, precision=PRECISE)
    outputs = jnp.einsum("hncd,hnde->hnce", query_decay, starts, precision=PRECISE) + jnp.einsum(
        "hnij,hnje->hnie", scores, fresh, precision=PRECISE
    )
    raw_mix = outputs.transpose(1, 2, 0, 3).reshape(length, head_count, width)
    return (
        raw_mix * lax.rsqrt(jnp.mean(raw_mix * raw_mix, -1, keepdims=True) + EPSILON) * norm_gain
    ).astype(jnp.bfloat16)


def experts_body(ffn_input, ffn_gain, expert_ids, expert_share, w_gate, w_up, w_down):
    floats = ffn_input.astype(jnp.float32)
    square_sum = of_everyone(jnp.sum(floats * floats, -1), TP)
    full_width = ffn_input.shape[1] * lax.axis_size(TP)
    normed = (floats * lax.rsqrt(square_sum / full_width + EPSILON)[:, None] * ffn_gain).astype(
        jnp.bfloat16
    )
    pick_count = expert_ids.shape[1]
    flat_ids = expert_ids.reshape(-1)
    sort_order = jnp.argsort(flat_ids, stable=True)
    source_rows = sort_order // pick_count
    experts_local = w_gate.shape[0]
    expert_devices = lax.axis_size("ep")
    capacity = flat_ids.shape[0] // (experts_local * expert_devices)
    outgoing = normed[source_rows].reshape(expert_devices, experts_local, capacity, normed.shape[1])
    arrived = lax.all_to_all(outgoing, "ep", split_axis=0, concat_axis=0, tiled=True)
    slab_in = gather_directly(arrived, TP, 3)
    gate_sum = jnp.einsum("secl,elf->secf", slab_in, w_gate, preferred_element_type=jnp.float32)
    up_sum = jnp.einsum("secl,elf->secf", slab_in, w_up, preferred_element_type=jnp.float32)
    hidden = (jax.nn.silu(gate_sum) * up_sum).astype(jnp.bfloat16)
    merged = jnp.einsum(
        "secf,efd->secd", gather_axes(hidden, TP, 3), w_down, preferred_element_type=jnp.float32
    )
    copies = merged.astype(jnp.bfloat16)
    returned = lax.all_to_all(copies, "ep", split_axis=0, concat_axis=0, tiled=True).reshape(
        -1, w_down.shape[2]
    )
    slots = jnp.argsort(sort_order)
    per_slot = returned[slots].reshape(expert_ids.shape[0], pick_count, -1)
    return jnp.sum(per_slot.astype(jnp.float32) * expert_share[..., None], axis=1).astype(
        jnp.bfloat16
    )


def body(
    mix_query,
    mix_keys,
    mix_values,
    beta_in,
    decay_in,
    norm_gain,
    ffn_input,
    ffn_gain,
    expert_ids,
    expert_share,
    w_gate,
    w_up,
    w_down,
):
    mix_out = mixer_body(mix_query, mix_keys, mix_values, beta_in, decay_in, norm_gain)
    ffn_out = experts_body(ffn_input, ffn_gain, expert_ids, expert_share, w_gate, w_up, w_down)
    return (mix_out, ffn_out)


def solution(mesh):
    torus = Mesh(
        mesh.devices.reshape(mesh.shape["grp"], mesh.shape["ep"], 8, 2),
        ("grp", "ep", "tp_0", "tp_1"),
    )
    in_specs = (
        P(("grp", "ep"), TP, None),
        P(("grp", "ep"), TP, None),
        P(("grp", "ep"), TP, None),
        P(TP, ("grp", "ep")),
        P(TP, ("grp", "ep")),
        P(),
        P(("grp", "ep"), TP),
        P(TP),
        P(("grp", "ep"), None),
        P(("grp", "ep"), None),
        P("ep", None, TP),
        P("ep", None, TP),
        P("ep", None, TP),
    )
    out_specs = (P(("grp", "ep"), TP, None), P(("grp", "ep"), TP))
    return jax.shard_map(body, mesh=torus, in_specs=in_specs, out_specs=out_specs, check_vma=False)
```

profile of v0, /device:TPU:80, one launch (start us, length us, event | category | flops | bytes accessed | tf_op | source)
XLA Modules:
  0.0 234.4 jit_solution(1865883967722144098)
XLA Ops:
  8.7 1.1 fusion.32
  9.7 1.0 convert_multiply_fusion
  16.7 1.1 fusion.10
  19.9 1.1 convolution_bitcast_fusion.1
  22.3 1.0 fusion.15
  24.3 2.1 pad.48
  29.0 7.6 %all-to-all-start = ((f32[16,1,128]{2,1,0:T(1,128)}), f32[16,1,128]{2,1,0:T(1,128)S(1)}, u32[]{:S(2)}, u32[]{:S(2)}) async-start(f32[16,1,128]{2,1,0:T(1,128)} %broadcast_in_dim.128), calls=%async_computation | async-start | bytes 16384 | tf_op jit(solution)/shard_map/all_to_all | solution.py:24
  36.9 3.2 %sort.34 = (s32[256]{0:T(256)}, s32[256]{0:T(256)S(1)}) sort(s32[256]{0:T(256)S(1)} %reshape.349, s32[256]{0:T(256)S(1)} %iota.67), dimensions={0}, to_apply=%region_8.9 | sort | flops 2048 | bytes 4096 | tf_op jit(solution)/shard_map/jit(argsort)/sort | solution.py:156
  40.1 3.2 %sort.35 = (s32[256]{0:T(256)}, s32[256]{0:T(256)S(1)}) sort(s32[256]{0:T(256)S(1)} %get-tuple-element.99, s32[256]{0:T(256)S(1)} %iota.68), dimensions={0}, to_apply=%region_9.10 | sort | flops 2048 | bytes 4096 | tf_op jit(solution)/shard_map/jit(argsort)/sort | solution.py:174
  44.1 1.8 gather_fusion
  45.9 43.7 %all-to-all-start.1 = ((bf16[16,1,16,256]{3,2,1,0:T(8,128)(2,1)}), bf16[16,1,16,256]{3,2,1,0:T(8,128)(2,1)S(1)}, u32[]{:S(2)}, u32[]{:S(2)}) async-start(bf16[16,1,16,256]{3,2,1,0:T(8,128)(2,1)} %bitcast.40), calls=%async_computation.1 | async-start | bytes 262144 | tf_op jit(solution)/shard_map/all_to_all | solution.py:162
  90.1 2.0 pad.66
  93.2 1.3 fusion.11
  94.4 10.1 %all-to-all-done.1 = bf16[16,1,16,256]{3,2,1,0:T(8,128)(2,1)S(1)} async-done(((bf16[16,1,16,256]{3,2,1,0:T(8,128)(2,1)}), bf16[16,1,16,256]{3,2,1,0:T(8,128)(2,1)S(1)}, u32[]{:S(2)}, u32[]{:S(2)}) %all-to-all-start.1) | async-done | bytes 131104 | tf_op jit(solution)/shard_map/all_to_all | solution.py:162
  104.6 1.6 broadcast_in_dim.131
  106.1 6.9 %all-to-all-start.2 = ((bf16[16,16,1,16,256]{4,3,1,2,0:T(8,128)(2,1)}), bf16[16,16,1,16,256]{4,3,1,2,0:T(8,128)(2,1)S(1)}, u32[]{:S(2)}, u32[]{:S(2)}) async-start(bf16[16,16,1,16,256]{4,3,1,2,0:T(8,128)(2,1)} %broadcast_in_dim.131), calls=%async_computation.2 | async-start | bytes 4194304 | tf_op jit(solution)/shard_map/all_to_all | solution.py:24
  113.0 28.3 %all-gather.2.cloned.1.call-done = f32[16,2,128,128]{3,2,1,0:T(8,128)} async-done(((f32[1,2,128,128]{3,2,1,0:T(8,128)}), f32[16,2,128,128]{3,2,1,0:T(8,128)}) %all-gather.2.cloned.1.call-update) | async-done | bytes 2097168 | tf_op jit(solution)/shard_map/all_gather | solution.py:18
  141.3 3.1 %fusion.105 = (f32[16,1,128,128]{3,2,1,0:T(8,128)}, f32[16,1,128,128]{3,2,1,0:T(8,128)}) fusion(f32[16,2,128,128]{3,2,1,0:T(8,128)} %all-gather.2.cloned.1.call-done), kind=kLoop, calls=%fused_computation.180 | loop fusion | bytes 4194304 | tf_op jit(solution)/shard_map/split | solution.py:19
  144.4 18.0 %while.14 = (s32[]{:T(128)}, f32[1,128,128]{2,1,0:T(8,128)S(1)}, s32[]{:T(128)}, f32[16,1,128,128]{3,2,1,0:T(8,128)}, f32[16,1,128,128]{3,2,1,0:T(8,128)}, /*index=5*/s32[]{:T(128)}, s32[]{:T(128)}) while((s32[]{:T(128)}, f32[1,128,128]{2,1,0:T(8,128)S(1)}, s32[]{:T(128)}, f32[16,1,128,128]{3,2,1,0:T(8,128)}, ...), condition=%wide.region_4.5_spmd.clone, body=%wide.region_3.4_spmd.clone.sunk | while | flops 25231364 | bytes 461407 | solution.py:134
  144.4 1.1 fusion.144
  145.5 1.1 fusion.144
  146.7 1.1 fusion.144
  147.8 1.1 fusion.144
  148.9 1.1 fusion.144
  150.0 1.1 fusion.144
  151.2 1.1 fusion.144
  152.3 1.1 fusion.144
  153.4 1.1 fusion.144
  154.5 1.1 fusion.144
  155.7 1.1 fusion.144
  156.8 1.1 fusion.144
  157.9 1.1 fusion.144
  159.0 1.1 fusion.144
  160.2 1.1 fusion.144
  161.3 1.1 fusion.144
  162.4 1.7 convolution_bitcast_fusion
  164.1 1.2 slice_add_fusion
  165.4 1.3 fusion.28
  166.7 1.3 convolution_subtract_fusion.1
  168.0 2.5 %copy.35 = bf16[16,1,16,16,256]{4,3,2,0,1:T(8,128)(2,1)} copy(bf16[16,1,16,16,256]{4,2,0,1,3:T(8,128)(2,1)S(1)} %bitcast.218) | data formatting | bytes 4194304 | tf_op jit(solution)/shard_map/transpose | solution.py:32
  170.5 2.9 %reshape.351 = bf16[16,16,4096]{2,1,0:T(8,128)(2,1)S(1)} reshape(bf16[16,1,16,16,256]{4,3,2,0,1:T(8,128)(2,1)} %copy.35) | data formatting | bytes 4194304 | tf_op jit(solution)/shard_map/reshape.56
  175.5 2.2 all_gather.10
  178.2 26.0 %all_gather.11 = bf16[16,1,16,1024]{3,2,0,1:T(8,128)(2,1)S(1)} all-gather(bf16[16,1,16,128]{3,2,0,1:T(8,128)(2,1)S(1)} %copy.37), channel_id=1, replica_groups=mesh['grp'=2,'ep'=16,'tp_0'=8,'tp_1'=2] {'tp_0'}, dimensions={3}, use_global_device_ids=true | all-gather | bytes 589824 | tf_op jit(solution)/shard_map/all_gather | solution.py:45
  204.2 0.9 fusion.16
  205.2 7.0 %all-to-all-start.3 = ((bf16[16,1,16,256]{3,2,1,0:T(8,128)(2,1)}), bf16[16,1,16,256]{3,2,1,0:T(8,128)(2,1)S(1)}, u32[]{:S(2)}, u32[]{:S(2)}) async-start(bf16[16,1,16,256]{3,2,1,0:T(8,128)(2,1)} %fusion.16), calls=%async_computation.3 | async-start | bytes 262144 | tf_op jit(solution)/shard_map/all_to_all | solution.py:171
  213.6 11.5 %all-to-all-done.3 = bf16[16,1,16,256]{3,2,1,0:T(8,128)(2,1)S(1)} async-done(((bf16[16,1,16,256]{3,2,1,0:T(8,128)(2,1)}), bf16[16,1,16,256]{3,2,1,0:T(8,128)(2,1)S(1)}, u32[]{:S(2)}, u32[]{:S(2)}) %all-to-all-start.3) | async-done | bytes 131104 | tf_op jit(solution)/shard_map/all_to_all | solution.py:171
  225.1 1.3 gather_fusion.1
  226.5 1.0 multiply_reduce_fusion
  (152 shorter events, 20.4 us)
Async XLA Ops:
  7.2 197.1 %copy-start = (bf16[1,1024,256]{2,1,0:T(8,128)(2,1)S(1)}, bf16[1,1024,256]{2,1,0:T(8,128)(2,1)}, u32[]{:S(2)}) copy-start(bf16[1,1024,256]{2,1,0:T(8,128)(2,1)} %param.27) | copy-start | bytes 1572868
  7.2 134.1 %all-gather.2.cloned.1.call-start = ((), (), s32[]{:S(2)}) async-start(), calls=%async_computation.4 | async-start | bytes 2228224 | tf_op jit(solution)/shard_map/all_gather | solution.py:18
  16.0 0.7 copy-start.2
  18.2 1.3 copy-start.17
  19.9 2.3 copy-start.4
  21.0 2.3 copy-start.9
  23.4 0.8 slice-start
  23.4 1.0 copy-start.13
  23.4 4.8 %copy-start.16 = (bf16[128,256]{1,0:T(8,128)(2,1)S(1)}, bf16[128,256]{1,0:T(8,128)(2,1)}, u32[]{:S(2)}) copy-start(bf16[128,256]{1,0:T(8,128)(2,1)} %param.21) | copy-start | bytes 196612
  23.5 13.2 %copy-start.18 = (s32[128,2]{0,1:T(2,128)S(1)}, s32[128,2]{0,1:T(2,128)}, u32[]{:S(2)}) copy-start(s32[128,2]{0,1:T(2,128)} %param.23) | copy-start | bytes 3076
  23.5 19.8 %copy-start.14 = (bf16[512,1,128]{2,0,1:T(8,128)(2,1)S(1)}, bf16[512,1,128]{2,0,1:T(8,128)(2,1)}, u32[]{:S(2)}) copy-start(bf16[512,1,128]{2,0,1:T(8,128)(2,1)} %param.15) | copy-start | bytes 393220
  23.5 20.5 %copy-start.19 = (f32[256]{0:T(256)S(1)}, f32[256]{0:T(256)}, u32[]{:S(2)}) copy-start(f32[256]{0:T(256)} %param.22) | copy-start | bytes 3076
  24.3 19.6 %copy-start.1 = (f32[1,8,128,128]{3,2,1,0:T(8,128)}, f32[1,8,128,128]{3,2,1,0:T(8,128)S(1)}, u32[]{:S(2)}) copy-start(f32[1,8,128,128]{3,2,1,0:T(8,128)S(1)} %pad.42) | copy-start | bytes 1572868
  26.5 65.7 %copy-start.20 = (f32[128,2]{0,1:T(2,128)S(1)}, f32[128,2]{0,1:T(2,128)}, u32[]{:S(2)}) copy-start(f32[128,2]{0,1:T(2,128)} %param.24) | copy-start | bytes 3076
  26.5 67.9 %copy-start.8 = (f32[1,8,128,128]{3,2,1,0:T(8,128)}, f32[1,8,128,128]{3,2,1,0:T(8,128)S(1)}, u32[]{:S(2)}) copy-start(f32[1,8,128,128]{3,2,1,0:T(8,128)S(1)} %pad.49) | copy-start | bytes 1572868
  29.0 15.0 %all-to-all-start = ((f32[16,1,128]{2,1,0:T(1,128)}), f32[16,1,128]{2,1,0:T(1,128)S(1)}, u32[]{:S(2)}, u32[]{:S(2)}) async-start(f32[16,1,128]{2,1,0:T(1,128)} %broadcast_in_dim.128), calls=%async_computation | async-start | bytes 16384 | tf_op jit(solution)/shard_map/all_to_all | solution.py:24
  45.9 58.7 %all-to-all-start.1 = ((bf16[16,1,16,256]{3,2,1,0:T(8,128)(2,1)}), bf16[16,1,16,256]{3,2,1,0:T(8,128)(2,1)S(1)}, u32[]{:S(2)}, u32[]{:S(2)}) async-start(bf16[16,1,16,256]{3,2,1,0:T(8,128)(2,1)} %bitcast.40), calls=%async_computation.1 | async-start | bytes 262144 | tf_op jit(solution)/shard_map/all_to_all | solution.py:162
  92.4 0.7 copy-start.6
  106.1 61.9 %all-to-all-start.2 = ((bf16[16,16,1,16,256]{4,3,1,2,0:T(8,128)(2,1)}), bf16[16,16,1,16,256]{4,3,1,2,0:T(8,128)(2,1)S(1)}, u32[]{:S(2)}, u32[]{:S(2)}) async-start(bf16[16,16,1,16,256]{4,3,1,2,0:T(8,128)(2,1)} %broadcast_in_dim.131), calls=%async_computation.2 | async-start | bytes 4194304 | tf_op jit(solution)/shard_map/all_to_all | solution.py:24
  162.4 2.9 %copy-start.7 = (f32[512,1,128]{2,0,1:T(8,128)S(1)}, f32[512,1,128]{2,0,1:T(8,128)}, u32[]{:S(2)}) copy-start(f32[512,1,128]{2,0,1:T(8,128)} %copy-done.6) | copy-start | bytes 786436
  162.4 4.3 %copy-start.3 = (f32[8,64,128]{2,1,0:T(8,128)S(1)}, f32[8,64,128]{2,1,0:T(8,128)}, u32[]{:S(2)}) copy-start(f32[8,64,128]{2,1,0:T(8,128)} %copy-done.2) | copy-start | bytes 786436
  162.4 4.3 %copy-start.5 = (f32[8,64,128]{2,1,0:T(8,128)S(1)}, f32[8,64,128]{2,1,0:T(8,128)}, u32[]{:S(2)}) copy-start(f32[8,64,128]{2,1,0:T(8,128)} %copy-done.4) | copy-start | bytes 786436
  170.5 2.9 %copy-start.15 = (bf16[1,4096,64]{1,2,0:T(8,128)(2,1)S(1)}, bf16[1,4096,64]{1,2,0:T(8,128)(2,1)}, u32[]{:S(2)}) copy-start(bf16[1,4096,64]{1,2,0:T(8,128)(2,1)} %param.25) | copy-start | bytes 1572868
  173.5 1.0 copy-start.22
  175.2 36.9 %copy-start.10 = (f32[8,64,64]{2,1,0:T(8,128)S(1)}, f32[8,64,64]{2,1,0:T(8,128)}, u32[]{:S(2)}) copy-start(f32[8,64,64]{2,1,0:T(8,128)} %fusion.11) | copy-start | bytes 393220
  175.2 36.9 %copy-start.11 = (f32[8,64,128]{2,1,0:T(8,128)S(1)}, f32[8,64,128]{2,1,0:T(8,128)}, u32[]{:S(2)}) copy-start(f32[8,64,128]{2,1,0:T(8,128)} %convolution_subtract_fusion.1) | copy-start | bytes 786436
  175.2 36.9 %copy-start.12 = (f32[8,64,128]{2,1,0:T(8,128)S(1)}, f32[8,64,128]{2,1,0:T(8,128)}, u32[]{:S(2)}) copy-start(f32[8,64,128]{2,1,0:T(8,128)} %fusion.28) | copy-start | bytes 786436
  175.5 37.3 %copy-start.21 = (f32[128]{0:T(128)S(1)}, f32[128]{0:T(128)}, u32[]{:S(2)}) copy-start(f32[128]{0:T(128)} %param.20) | copy-start | bytes 1540
  205.2 19.9 %all-to-all-start.3 = ((bf16[16,1,16,256]{3,2,1,0:T(8,128)(2,1)}), bf16[16,1,16,256]{3,2,1,0:T(8,128)(2,1)S(1)}, u32[]{:S(2)}, u32[]{:S(2)}) async-start(bf16[16,1,16,256]{3,2,1,0:T(8,128)(2,1)} %fusion.16), calls=%async_computation.3 | async-start | bytes 262144 | tf_op jit(solution)/shard_map/all_to_all | solution.py:171
Sparse Core Ops, SparseCore 0:
  28.4 112.8 all-gather.1
where the time goes:
time: 236 us; the launch traced here: 234 us
  starting transfers between devices  65.2 us (28%)
  waiting for transfers between devices  50.4 us (21%)
  matrix products  36.9 us (16%)
  blocking collectives  28.3 us (12%)
  local copies, waits for them, and re-layouts  22.6 us (10%)
  other arithmetic  15.5 us (7%)
  between operations  14.9 us (6%)
    all_to_all x1, starting transfers between devices, experts_body(): lax.all_to_all(outgoing, 'ep', split_axis=0, concat_axis=0, tiled=True)  43.7 us
    all_gather x1, waiting for transfers between devices, sent_together(): result = lax.all_gather(both, axis, axis=dim, tiled=True)  28.3 us
    all_gather x2, blocking collectives, gather_axes(): result = lax.all_gather(result, axes[number], axis=dim, tiled=True)  28.3 us
    dot_general x16, matrix products, absorb(): jnp.matmul(all_maps[member], carried, precision=PRECISE) + all_adds[member]  17.3 us
    all_to_all x2, starting transfers between devices, from_everyone(): lax.all_to_all(jnp.broadcast_to(x[None], (size, *x.shape)), axis, 0, 0, t...  14.5 us
    all_to_all x1, waiting for transfers between devices, experts_body(): lax.all_to_all(copies, 'ep', split_axis=0, concat_axis=0, tiled=True)  11.5 us
    all_to_all x1, waiting for transfers between devices, experts_body(): lax.all_to_all(outgoing, 'ep', split_axis=0, concat_axis=0, tiled=True)  10.1 us
    all_to_all x1, starting transfers between devices, experts_body(): lax.all_to_all(copies, 'ep', split_axis=0, concat_axis=0, tiled=True)  6.97 us
  transfers between devices with their start and end apart: 5, of which 4 were waited for; matrix products, arithmetic and copies ran while one was open for 18% of the time, Pallas kernels for 0%

commit v1 on v0

v1 whole, which is shorter than its diff:
```python
import functools

import jax
import jax.numpy as jnp
from jax import lax
from jax.experimental import pallas as pl
from jax.experimental.pallas import tpu as pltpu
from jax.sharding import PartitionSpec as P

MESH = pl.DeviceIdType.MESH
EPSILON = 1e-06
BLOCK = 64
WIDE = 128
F32 = jnp.float32
BF16 = jnp.bfloat16

NN = ((1,), (0,))
NT = ((1,), (1,))
TN = ((0,), (0,))


def dot(a, b, dims=NN):
    return lax.dot_general(a, b, (dims, ((), ())), preferred_element_type=F32)


def halves(a):
    high = a.astype(BF16)
    return high, (a - high.astype(F32)).astype(BF16)


def dot_left(a, b, dims=NN):
    high, low = halves(a)
    return dot(high, b, dims) + dot(low, b, dims)


def dot_right(a, b, dims=NN):
    high, low = halves(b)
    return dot(a, high, dims) + dot(a, low, dims)


def dot_both(a, b, dims=NN):
    ah, al = halves(a)
    bh, bl = halves(b)
    return dot(ah, bh, dims) + (dot(ah, bl, dims) + dot(al, bh, dims))


def down_columns(row):
    return jnp.broadcast_to(row, (row.shape[1], row.shape[1])).T


def grid_of(n):
    return (
        lax.broadcasted_iota(jnp.int32, (n, n), 0),
        lax.broadcasted_iota(jnp.int32, (n, n), 1),
    )


def running_sums(rates):
    i, j = grid_of(WIDE)
    upper = jnp.where(i <= j, 1.0, 0.0).astype(BF16)
    high, rest = halves(rates)
    mid = (rates - high.astype(F32) - rest.astype(F32)).astype(BF16)
    return -(dot(high, upper) + (dot(rest, upper) + dot(mid, upper)))


def group_inverse(q, k, beta, cum):
    i, j = grid_of(WIDE)
    qf, kf = q.astype(F32), k.astype(F32)
    rq = lax.rsqrt(jnp.sum(qf * qf, -1, keepdims=True) + EPSILON) * (WIDE**-0.5)
    rk = lax.rsqrt(jnp.sum(kf * kf, -1, keepdims=True) + EPSILON)
    rk_row = jnp.broadcast_to(rk, (WIDE, WIDE)).T
    spread = jnp.where(i >= j, down_columns(cum) - cum, 0.0)
    decay = jnp.exp(spread) * rk_row
    lower = jnp.where(i > j, dot(k, k, NT) * rk * down_columns(beta) * decay, 0.0)
    scores = jnp.where(i >= j, dot(q, k, NT) * rq * decay, 0.0)
    same = (i // BLOCK) == (j // BLOCK)
    powered = jnp.where(same, -lower, 0.0)
    across = jnp.where(same, 0.0, lower)
    product = jnp.where(i == j, 1.0, 0.0) + powered
    for _ in range(1, (BLOCK - 1).bit_length()):
        powered = dot_both(powered, powered)
        product = product + dot_both(product, powered)
    inverse = product - dot_both(product, dot_both(across, product))
    return inverse, scores, rq, rk, rk_row[:1]


def group_terms(q, k, v, beta, cum, inverse, scores, rq, rk, rk_row):
    i, j = grid_of(WIDE)
    cum_col = down_columns(cum)[:, :1]
    last = cum[:, WIDE - 1 :]
    update = dot_left(inverse * beta, v)
    correction = dot_left(inverse * (beta * jnp.exp(cum) * rk_row), k)
    both = jnp.concatenate([update, correction], axis=1)
    moved = dot_right(k, both * (rk * jnp.exp(last - cum_col)), TN)
    shift = moved[:, :WIDE]
    transfer = jnp.where(i == j, jnp.exp(last), 0.0) - moved[:, WIDE:]
    seen = dot_both(scores, both)
    base = seen[:, :WIDE]
    reach = q.astype(F32) * (rq * jnp.exp(cum_col)) - seen[:, WIDE:]
    return shift, transfer, base, reach


def softplus(x):
    return jnp.maximum(x, 0.0) + jnp.log1p(jnp.exp(-jnp.abs(x)))


def dispatch_tables(ids, capacity, experts):
    tokens = ids.shape[1]
    lane = lax.broadcasted_iota(jnp.int32, (tokens, WIDE), 1)
    first = jnp.broadcast_to(ids[0:1].astype(F32), (tokens, tokens)).T.astype(jnp.int32)[:, :WIDE]
    second = jnp.broadcast_to(ids[1:2].astype(F32), (tokens, tokens)).T.astype(jnp.int32)[:, :WIDE]
    one = jnp.where(lane == first, 1.0, 0.0)
    two = jnp.where(lane == second, 1.0, 0.0)
    i, j = grid_of(tokens)
    before = jnp.where(i > j, 1.0, 0.0).astype(BF16)
    rank = dot(before, (one + two).astype(BF16)) + (lane * capacity).astype(F32)
    slot_one = jnp.sum(one * rank, -1, keepdims=True).astype(jnp.int32)
    slot_two = jnp.sum(two * rank, -1, keepdims=True).astype(jnp.int32)
    return slot_one, slot_two


def program_kernel(nz, nx, *refs):
    (
        q_in, k_in, v_in, beta_in, decay_in, ng_in, x_in, gain_in, ids_in, share_in,
        wg_in, wu_in, wd_in, mix_out, ffn_out,
        q_s, k_s, v_s, beta_s, decay_s, ng_s, x_s, gains, ids_s, share_s, wt, wd,
        rows_s, xs, xg, hg, ret, got, comm, base_s, reach_s, qm, sf, sb, mo_s, fo_s,
        load_sem, disp_send, disp_recv, x_send, x_recv, hid_send, hid_recv,
        ret_send, ret_recv, g_send, g_recv, w_send, w_recv, f_send, f_recv, b_send, b_recv,
    ) = refs
    grp, z, tp = lax.axis_index("grp"), lax.axis_index("ep"), lax.axis_index("tp")
    x, c = tp // 2, tp % 2
    partner = 2 * x + 1 - c
    tokens, feats = x_s.shape
    capacity = xs.shape[1]
    hid = wg_in.shape[0]
    groups = q_s.shape[0] // WIDE
    sources = nz // 2
    parity = z % 2
    mine = z // 2
    waits = []

    def remote(src, dst, send, recv, zz, tt):
        return pltpu.make_async_remote_copy(
            src_ref=src, dst_ref=dst, send_sem=send, recv_sem=recv,
            device_id=(grp, zz, tt), device_id_type=MESH,
        )

    barrier = pltpu.get_barrier_semaphore()
    for dz in sorted(range(1, nz), key=lambda k: -min(k, nz - k)):
        for core in range(2):
            pl.semaphore_signal(
                barrier, inc=1, device_id=(grp, (z + dz) % nz, 2 * x + core), device_id_type=MESH
            )
    for dt in range(1, 2 * nx):
        pl.semaphore_signal(
            barrier, inc=1, device_id=(grp, z, (tp + dt) % (2 * nx)), device_id_type=MESH
        )

    places = [
        (x_in, x_s), (ids_in, ids_s), (beta_in, beta_s), (decay_in, decay_s), (k_in, k_s), (q_in, q_s),
        (v_in, v_s), (gain_in, gains.at[tp]), (share_in, share_s), (ng_in, ng_s),
        (wg_in, wt.at[pl.ds(pl.multiple_of(c * hid, hid), hid), :]),
        (wu_in, wt.at[pl.ds(pl.multiple_of((2 + c) * hid, hid), hid), :]),
        (wd_in, wd.at[c]),
    ]
    loads = [pltpu.make_async_copy(src, dst, load_sem.at[n]) for n, (src, dst) in enumerate(places)]
    for load in loads:
        load.start()

    loads[0].wait()
    loads[1].wait()
    slot_one, slot_two = dispatch_tables(ids_s[...], capacity, nz)
    slots = lax.broadcasted_iota(jnp.int32, (tokens, 2 * tokens), 1)
    chosen = jnp.where((slots == slot_one) | (slots == slot_two), 1.0, 0.0).astype(BF16)
    ordered = dot(chosen, x_s[...], TN).astype(BF16)
    for e in range(nz):
        xs[e] = ordered[e * capacity : (e + 1) * capacity]

    for n in (2, 3, 4, 5):
        loads[n].wait()
    for g in range(groups):
        cut = slice(g * WIDE, (g + 1) * WIDE)
        rows_s[0, g : g + 1, :] = 1.0 / (1.0 + jnp.exp(-beta_s[:, cut]))
        rows_s[1, g : g + 1, :] = softplus(decay_s[:, cut])
    for g in range(groups, 8):
        rows_s[1, g : g + 1, :] = jnp.zeros((1, WIDE), F32)
    rows_s[2] = running_sums(rows_s[1])
    firsts = []
    for g in range(groups):
        cut = slice(g * WIDE, (g + 1) * WIDE)
        beta, cum = rows_s[0, g : g + 1, :], rows_s[2, g : g + 1, :]
        firsts.append(group_inverse(q_s[cut], k_s[cut], beta, cum))

    pl.semaphore_wait(barrier, 2 * (nz - 1) + 2 * nx - 1)

    row_here = pl.ds(pl.multiple_of(mine * capacity, capacity), capacity)
    for dz in sorted(range(1, nz), key=lambda k: -min(k, nz - k)):
        e = (z + dz) % nz
        copy = remote(
            xs.at[e], xg.at[x, c, row_here, :], disp_send.at[dz], disp_recv.at[mine, c], e, 2 * x + parity
        )
        copy.start()
        waits.append((None, copy))
    own = remote(xs.at[z], xg.at[x, c, row_here, :], disp_send.at[0], disp_recv.at[mine, c], z, partner)

    @pl.when(parity != c)
    def _():
        own.start()

    waits.append((parity != c, own))

    @pl.when(parity == c)
    def _():
        xg[x, c, row_here, :] = xs[z]

    loads[7].wait()
    for dt in range(1, 2 * nx):
        copy = remote(gains.at[tp], gains.at[tp], g_send.at[dt], g_recv.at[dt], z, (tp + dt) % (2 * nx))
        copy.start()
        waits.append((None, copy))
    to_partner = []
    for n, (src, dst) in enumerate(places[10:]):
        copy = remote(src, dst, w_send.at[n], w_recv.at[n], z, partner)
        copy.start()
        waits.append((None, copy))
        to_partner.append(copy)

    loads[6].wait()
    total = None
    for g in range(groups):
        cut = slice(g * WIDE, (g + 1) * WIDE)
        beta, cum = rows_s[0, g : g + 1, :], rows_s[2, g : g + 1, :]
        shift, transfer, base, reach = group_terms(q_s[cut], k_s[cut], v_s[cut], beta, cum, *firsts[g])
        if total is None:
            total = jnp.concatenate([shift, transfer], axis=1)
        else:
            through = dot_both(reach, total)
            base = base + through[:, :WIDE]
            reach = through[:, WIDE:]
            total = dot_both(transfer, total)
            total = jnp.concatenate([total[:, :WIDE] + shift, total[:, WIDE:]], axis=1)
        base_s[cut, :] = base
        reach_s[cut, :] = reach
    comm[z] = total.astype(BF16)
    i, j = grid_of(WIDE)
    qm[...] = jnp.where(i == j, 1.0, 0.0)
    sf[...] = jnp.zeros_like(sf)
    sb[...] = jnp.zeros_like(sb)
    ahead = nz // 2
    behind = nz - 1 - ahead
    wrapped = nz - 1 - ahead

    def pass_forward(step, owner, condition):
        copy = remote(comm.at[owner], comm.at[owner], f_send.at[step], f_recv.at[step], (z + 1) % nz, tp)

        @pl.when(condition)
        def _():
            copy.start()

        waits.append((condition, copy))

    def pass_backward(step, owner, condition):
        copy = remote(
            comm.at[owner], comm.at[owner], b_send.at[step], b_recv.at[step], (z + nz - 1) % nz, tp
        )

        @pl.when(condition)
        def _():
            copy.start()

        waits.append((condition, copy))

    pass_forward(1, z, z + 1 < nz)
    pass_backward(1, z, z < wrapped)

    def map_step(d):
        if d <= ahead:
            owner = (z + nz - d) % nz
            fits = z >= d
            arrival = remote(
                comm.at[owner], comm.at[owner], f_send.at[d], f_recv.at[d], (z + 1) % nz, tp
            )

            @pl.when(fits)
            def _():
                arrival.wait_recv()

            if d < ahead:
                pass_forward(d + 1, owner, jnp.logical_and(fits, z + 1 < nz))

        if d <= behind:
            owner_back = (z + d) % nz
            fits_back = owner_back < wrapped
            arrival_back = remote(
                comm.at[owner_back], comm.at[owner_back], b_send.at[d], b_recv.at[d], (z + 1) % nz, tp
            )

            @pl.when(fits_back)
            def _():
                arrival_back.wait_recv()

            if d < behind:
                pass_backward(d + 1, owner_back, fits_back)

        if d <= ahead:

            @pl.when(fits)
            def _():
                advanced = dot_left(qm[...], comm[owner])
                sf[...] += advanced[:, :WIDE]
                qm[...] = advanced[:, WIDE:]

        if d <= behind:

            @pl.when(jnp.logical_and(fits_back, z + d >= nz))
            def _():
                message = comm[owner_back]
                sb[...] = dot_right(message[:, WIDE:], sb[...]) + message[:, :WIDE].astype(F32)

    pieces = min(4, sources)
    per_piece = sources // pieces
    piece_rows = per_piece * capacity
    distance = nx // 2
    order = [0] + [o for k in range(1, pieces) for o in (k, pieces - k) if k <= pieces - k]
    order = list(dict.fromkeys(order))
    where = [(z // (2 * per_piece) + o) % pieces for o in order]

    def piece_of(chip, n):
        rows = pl.ds(pl.multiple_of(where[n] * piece_rows, piece_rows), piece_rows)
        return xg.at[chip, :, rows, :]

    def travels(way, d):
        if d < distance:
            return range(pieces)
        return range(pieces // 2) if way == 0 else range(pieces // 2, pieces)

    def ring(way, d, n):
        chip = (x + nx - (d - 1)) % nx if way == 0 else (x + d - 1) % nx
        to = (x + 1) % nx if way == 0 else (x + nx - 1) % nx
        return remote(
            piece_of(chip, n), piece_of(chip, n), x_send.at[way, d, n], x_recv.at[way, d, n], z, 2 * to + c
        )

    def arrived(way, d, n):
        chip = (x + nx - d) % nx if way == 0 else (x + d) % nx
        to = (x + 1) % nx if way == 0 else (x + nx - 1) % nx
        return remote(
            piece_of(chip, n), piece_of(chip, n), x_send.at[way, d, n], x_recv.at[way, d, n], z, 2 * to + c
        )

    for n in range(pieces):
        for t in range(per_piece):
            m = where[n] * per_piece + t
            for core in range(2):
                rows = pl.ds(pl.multiple_of(m * capacity, capacity), capacity)
                landing = xg.at[x, core, rows, :]
                arrival = remote(landing, landing, disp_send.at[0], disp_recv.at[m, core], z, partner)

                @pl.when(jnp.logical_or(2 * m + c != z, core != c))
                def _():
                    arrival.wait_recv()

        for way in range(2):
            if n in travels(way, 1):
                copy = ring(way, 1, n)
                copy.start()
                waits.append((None, copy))

    for load in loads[8:]:
        load.wait()
    for n in range(3):
        to_partner[n].wait_recv()
    for dt in range(1, 2 * nx):
        sender = (tp + 2 * nx - dt) % (2 * nx)
        remote(gains.at[sender], gains.at[sender], g_send.at[dt], g_recv.at[dt], z, sender).wait_recv()

    def products(chip, acc, squares):
        for core in range(2):
            part = xg[chip, core].astype(F32)
            squares = squares + jnp.sum(part * part, -1, keepdims=True)
            member = 2 * chip + core
            scaled = (part * gains[member]).astype(BF16)
            columns = pl.ds(pl.multiple_of(member * feats, feats), feats)
            acc = acc + dot(scaled, wt[:, columns], NT)
        return acc, squares

    rows_all = sources * capacity
    acc = jnp.zeros((rows_all, 4 * hid), F32)
    squares = jnp.zeros((rows_all, 1), F32)
    acc, squares = products(x, acc, squares)
    for d in range(1, distance + 1):
        for n in range(pieces):
            for way in range(2):
                if n in travels(way, d):
                    arrived(way, d, n).wait_recv()
                    if d < distance and n in travels(way, d + 1):
                        copy = ring(way, d + 1, n)
                        copy.start()
                        waits.append((None, copy))
        map_step(d)
        acc, squares = products((x + nx - d) % nx, acc, squares)
        if d < distance:
            acc, squares = products((x + d) % nx, acc, squares)

    scale = lax.rsqrt(squares / (feats * 2 * nx) + EPSILON)
    gate = acc[:, : 2 * hid] * scale
    up = acc[:, 2 * hid :] * scale
    hg[x] = (gate / (1.0 + jnp.exp(-gate)) * up).astype(BF16)
    for dx in sorted(range(1, nx), key=lambda k: -min(k, nx - k)):
        copy = remote(hg.at[x], hg.at[x], hid_send.at[dx], hid_recv.at[dx], z, 2 * ((x + dx) % nx) + c)
        copy.start()
        waits.append((None, copy))
    done = distance
    for d in range(done + 1, min(done + 3, ahead + 1)):
        map_step(d)
        done = d
    for dx in range(1, nx):
        chip = (x + nx - dx) % nx
        remote(hg.at[chip], hg.at[chip], hid_send.at[dx], hid_recv.at[dx], z, 2 * chip + c).wait_recv()
    hidden = jnp.concatenate([hg[n] for n in range(nx)], axis=1)
    for core in range(2):
        ret[core] = dot(hidden, wd[core]).astype(BF16)

    slot_here = pl.ds(pl.multiple_of(z * capacity, capacity), capacity)
    for dm in sorted(range(sources), key=lambda k: -min(k, sources - k)):
        m = (mine + dm) % sources
        rows = pl.ds(pl.multiple_of(m * capacity, capacity), capacity)
        target = 2 * m + c
        for core in range(2):
            copy = remote(
                ret.at[core, rows, :], got.at[slot_here, :], ret_send.at[dm, core], ret_recv.at[z],
                target, 2 * x + core,
            )
            away = jnp.logical_or(target != z, core != c)

            @pl.when(away)
            def _():
                copy.start()

            waits.append((away, copy))

            @pl.when(jnp.logical_not(away))
            def _():
                got[slot_here, :] = ret[core, rows, :]

    for d in range(done + 1, ahead + 1):
        map_step(d)
    entering = sf[...] + dot_both(qm[...], sb[...])
    for g in range(groups):
        cut = slice(g * WIDE, (g + 1) * WIDE)
        raw = base_s[cut, :] + dot_both(reach_s[cut, :], entering)
        norm = lax.rsqrt(jnp.mean(raw * raw, -1, keepdims=True) + EPSILON)
        mo_s[cut, :] = (raw * norm * ng_s[...]).astype(BF16)
    store_mix = pltpu.make_async_copy(mo_s, mix_out, load_sem.at[13])
    store_mix.start()

    shares = share_s[...]
    first = jnp.broadcast_to(shares[0:1], (tokens, tokens)).T[:, :1]
    second = jnp.broadcast_to(shares[1:2], (tokens, tokens)).T[:, :1]
    weights = jnp.where(slots == slot_one, first, 0.0) + jnp.where(slots == slot_two, second, 0.0)
    for e in range(nz):
        landing = got.at[pl.ds(e * capacity, capacity), :]
        arrival = remote(landing, landing, disp_send.at[0], ret_recv.at[e], z, partner)

        @pl.when(jnp.logical_or(e != z, parity != c))
        def _():
            arrival.wait_recv()

    fo_s[...] = dot_left(weights, got[...]).astype(BF16)
    store_ffn = pltpu.make_async_copy(fo_s, ffn_out, load_sem.at[14])
    store_ffn.start()
    for condition, copy in waits:
        if condition is None:
            copy.wait_send()
        else:

            @pl.when(condition)
            def _():
                copy.wait_send()

    store_mix.wait()
    store_ffn.wait()


def body(nz, nx, mix_query, mix_keys, mix_values, beta_in, decay_in, norm_gain, ffn_input, ffn_gain,
         expert_ids, expert_share, w_gate, w_up, w_down):
    length, _, width = mix_query.shape
    tokens, feats = ffn_input.shape
    hid = w_gate.shape[2]
    full = w_gate.shape[1]
    capacity = 2 * tokens // nz
    rows = nz // 2 * capacity
    ff = w_down.shape[1]
    dma = pltpu.SemaphoreType.DMA
    vmem = pltpu.VMEM
    call = pl.pallas_call(
        functools.partial(program_kernel, nz, nx),
        out_shape=(
            jax.ShapeDtypeStruct((length, width), BF16),
            jax.ShapeDtypeStruct((tokens, feats), BF16),
        ),
        in_specs=[pl.BlockSpec(memory_space=pl.ANY)] * 13,
        out_specs=[pl.BlockSpec(memory_space=pl.ANY)] * 2,
        scratch_shapes=[
            vmem((length, width), BF16), vmem((length, width), BF16), vmem((length, width), BF16),
            vmem((1, length), F32), vmem((1, length), F32), vmem((1, width), F32),
            vmem((tokens, feats), BF16), vmem((2 * nx, 1, feats), F32),
            vmem((2, tokens), jnp.int32), vmem((2, tokens), F32),
            vmem((4 * hid, full), BF16), vmem((2, ff, feats), BF16),
            vmem((3, 8, width), F32),
            vmem((nz, capacity, feats), BF16),
            vmem((nx, 2, rows, feats), BF16),
            vmem((nx, rows, 2 * hid), BF16),
            vmem((2, rows, feats), BF16),
            vmem((2 * tokens, feats), BF16),
            vmem((nz, width, 2 * width), BF16),
            vmem((length, width), F32), vmem((length, width), F32),
            vmem((width, width), F32), vmem((width, width), F32), vmem((width, width), F32),
            vmem((length, width), BF16), vmem((tokens, feats), BF16),
            dma((15,)), dma((nz,)), dma((nz // 2, 2)),
            dma((2, nx // 2 + 1, 4)), dma((2, nx // 2 + 1, 4)),
            dma((nx,)), dma((nx,)),
            dma((nz // 2, 2)), dma((nz,)),
            dma((2 * nx,)), dma((2 * nx,)), dma((3,)), dma((3,)),
            dma((nz // 2 + 1,)), dma((nz // 2 + 1,)), dma((nz // 2 + 1,)), dma((nz // 2 + 1,)),
        ],
        compiler_params=pltpu.CompilerParams(collective_id=0, has_side_effects=True),
    )
    mix, ffn = call(
        mix_query.reshape(length, width), mix_keys.reshape(length, width), mix_values.reshape(length, width),
        beta_in, decay_in, norm_gain.reshape(1, width), ffn_input, ffn_gain.reshape(1, feats),
        expert_ids.T, expert_share.T, w_gate[0].T, w_up[0].T, w_down[0],
    )
    return mix.reshape(length, 1, width), ffn


def solution(mesh):
    nz, nx = mesh.shape["ep"], mesh.shape["tp"] // 2
    in_specs = (
        P(("grp", "ep"), "tp", None), P(("grp", "ep"), "tp", None), P(("grp", "ep"), "tp", None),
        P("tp", ("grp", "ep")), P("tp", ("grp", "ep")), P(),
        P(("grp", "ep"), "tp"), P("tp"), P(("grp", "ep"), None), P(("grp", "ep"), None),
        P("ep", None, "tp"), P("ep", None, "tp"), P("ep", None, "tp"),
    )
    out_specs = (P(("grp", "ep"), "tp", None), P(("grp", "ep"), "tp"))
    return jax.shard_map(
        functools.partial(body, nz, nx), mesh=mesh, in_specs=in_specs, out_specs=out_specs, check_vma=False
    )
```

time: 236 us -> 96.7 us (0.41)
  Pallas kernels: 0 us -> 92.7 us
  starting transfers between devices: 65.2 us -> 0 us
  waiting for transfers between devices: 50.4 us -> 0 us
  matrix products: 36.9 us -> 0 us
  blocking collectives: 28.3 us -> 0 us
  local copies, waits for them, and re-layouts: 22.6 us -> 2.23 us
  other arithmetic: 15.5 us -> 0 us
  between operations: 14.9 us -> 0.65 us
    pallas_call x0 -> x1, Pallas kernels: none -> 92.7 us  [body(): call(mix_query.reshape(length, width), mix_keys.reshape(length, width), m...]
    all_to_all x4 -> x0, starting transfers between devices: 65.2 us -> none  [the longest x1 43.7 us: experts_body(): lax.all_to_all(outgoing, 'ep', split_axis=0, concat_axis=0, tiled=True)]
    dot_general x49 -> x0, matrix products: 36.9 us -> none  [the longest x16 17.3 us: absorb(): jnp.matmul(all_maps[member], carried, precision=PRECISE) + all_adds[member]]
    all_gather x1 -> x0, waiting for transfers between devices: 28.3 us -> none  [sent_together(): result = lax.all_gather(both, axis, axis=dim, tiled=True)]
    all_gather x2 -> x0, blocking collectives: 28.3 us -> none  [gather_axes(): result = lax.all_gather(result, axes[number], axis=dim, tiled=True)]
    all_to_all x4 -> x0, waiting for transfers between devices: 22 us -> none  [the longest x1 11.5 us: experts_body(): lax.all_to_all(copies, 'ep', split_axis=0, concat_axis=0, tiled=True)]
    sort x2 -> x0, other arithmetic: 6.39 us -> none  [the longest x1 3.19 us: experts_body(): slots = jnp.argsort(sort_order)]
    split x1 -> x0, local copies, waits for them, and re-layouts: 3.1 us -> none  [sent_together(): jnp.split(result, [sum(widths[:k]) for k in range(1, len(widths))], axis=...]
  transfers between devices with their start and end apart: 5 -> 0, of which waited for: 4 -> 0; matrix products, arithmetic and copies ran while one was open for 18% -> 0% of each run, Pallas kernels for 0% -> 0%
where the time goes in v1:
time: 96.7 us; the launch traced here: 95.6 us
  Pallas kernels  92.7 us (96%)
  local copies, waits for them, and re-layouts  2.23 us (2%)
    pallas_call x1, Pallas kernels, body(): call(mix_query.reshape(length, width), mix_keys.reshape(length, width), m...  92.7 us
    unnamed x4, local copies, waits for them, and re-layouts  2.23 us

profile of v1, /device:TPU:80, one launch (start us, length us, event | category | flops | bytes accessed | tf_op | source)
XLA Modules:
  0.0 95.6 jit_solution(17949148237010649154)
XLA Ops:
  0.6 92.7 %shard_map.140 = (bf16[512,128]{1,0:T(8,128)(2,1)}, bf16[128,256]{1,0:T(8,128)(2,1)}) custom-call(bf16[512,128]{1,0:T(8,128)(2,1)} %bitcast.18, bf16[512,128]{1,0:T(8,128)(2,1)} %bitcast.19, bf16[512,128]{1,0:T(8,128)(2,1)} %bitcast.20, f32[1,512]{1,0:T(1,128)} %refs_3_.1, f32[1,512]{1,0:T(1,128)} %refs_4_.1, f32[1,128]{1,0:T(1,128)} %bitcast.25, ...), custom_call_target="tpu_custom_call" | custom-call | tf_op jit(solution)/shard_map/pallas_call | solution.py:530
  93.4 0.0 copy-start
  93.4 1.6 %copy.17 = bf16[512,1,128]{2,0,1:T(8,128)(2,1)} copy(bf16[512,1,128]{2,0,1:T(8,128)(2,1)} %bitcast.21) | data formatting | bytes 262144
  95.0 0.0 copy-done
  95.0 0.6 copy.18
Async XLA Ops:
  93.4 1.6 %copy-start = (bf16[128,256]{1,0:T(8,128)(2,1)S(1)}, bf16[128,256]{1,0:T(8,128)(2,1)}, u32[]{:S(2)}) copy-start(bf16[128,256]{1,0:T(8,128)(2,1)} %get-tuple-element.9) | copy-start | bytes 196612

commit v2 on v1

v2 whole, which is shorter than its diff:
```python
import functools

import jax
import jax.numpy as jnp
from jax import lax
from jax.experimental import pallas as pl
from jax.experimental.pallas import tpu as pltpu
from jax.sharding import PartitionSpec as P

MESH = pl.DeviceIdType.MESH
EPSILON = 1e-06
BLOCK = 64
WIDE = 128
F32 = jnp.float32
BF16 = jnp.bfloat16

NN = ((1,), (0,))
NT = ((1,), (1,))
TN = ((0,), (0,))


def dot(a, b, dims=NN):
    return lax.dot_general(a, b, (dims, ((), ())), preferred_element_type=F32)


def halves(a):
    high = a.astype(BF16)
    return high, (a - high.astype(F32)).astype(BF16)


def dot_left(a, b, dims=NN):
    high, low = halves(a)
    return dot(high, b, dims) + dot(low, b, dims)


def dot_right(a, b, dims=NN):
    high, low = halves(b)
    return dot(a, high, dims) + dot(a, low, dims)


def dot_both(a, b, dims=NN):
    ah, al = halves(a)
    bh, bl = halves(b)
    return dot(ah, bh, dims) + (dot(ah, bl, dims) + dot(al, bh, dims))


def down_columns(row):
    return jnp.broadcast_to(row, (row.shape[1], row.shape[1])).T


def grid_of(n):
    return (
        lax.broadcasted_iota(jnp.int32, (n, n), 0),
        lax.broadcasted_iota(jnp.int32, (n, n), 1),
    )


def running_sums(rates):
    i, j = grid_of(WIDE)
    upper = jnp.where(i <= j, 1.0, 0.0).astype(BF16)
    high, rest = halves(rates)
    mid = (rates - high.astype(F32) - rest.astype(F32)).astype(BF16)
    return -(dot(high, upper) + (dot(rest, upper) + dot(mid, upper)))


def group_inverse(q, k, beta, cum):
    i, j = grid_of(WIDE)
    qf, kf = q.astype(F32), k.astype(F32)
    rq = lax.rsqrt(jnp.sum(qf * qf, -1, keepdims=True) + EPSILON) * (WIDE**-0.5)
    rk = lax.rsqrt(jnp.sum(kf * kf, -1, keepdims=True) + EPSILON)
    rk_row = jnp.broadcast_to(rk, (WIDE, WIDE)).T
    spread = jnp.where(i >= j, down_columns(cum) - cum, 0.0)
    decay = jnp.exp(spread) * rk_row
    lower = jnp.where(i > j, dot(k, k, NT) * rk * down_columns(beta) * decay, 0.0)
    scores = jnp.where(i >= j, dot(q, k, NT) * rq * decay, 0.0)
    same = (i // BLOCK) == (j // BLOCK)
    powered = jnp.where(same, -lower, 0.0)
    across = jnp.where(same, 0.0, lower)
    product = jnp.where(i == j, 1.0, 0.0) + powered
    for _ in range(1, (BLOCK - 1).bit_length()):
        powered = dot_both(powered, powered)
        product = product + dot_both(product, powered)
    inverse = product - dot_both(product, dot_both(across, product))
    return inverse, scores, rq, rk, rk_row[:1]


def group_terms(q, k, v, beta, cum, inverse, scores, rq, rk, rk_row):
    i, j = grid_of(WIDE)
    cum_col = down_columns(cum)[:, :1]
    last = cum[:, WIDE - 1 :]
    update = dot_left(inverse * beta, v)
    correction = dot_left(inverse * (beta * jnp.exp(cum) * rk_row), k)
    both = jnp.concatenate([update, correction], axis=1)
    moved = dot_right(k, both * (rk * jnp.exp(last - cum_col)), TN)
    shift = moved[:, :WIDE]
    transfer = jnp.where(i == j, jnp.exp(last), 0.0) - moved[:, WIDE:]
    seen = dot_both(scores, both)
    base = seen[:, :WIDE]
    reach = q.astype(F32) * (rq * jnp.exp(cum_col)) - seen[:, WIDE:]
    return shift, transfer, base, reach


def softplus(x):
    return jnp.maximum(x, 0.0) + jnp.log1p(jnp.exp(-jnp.abs(x)))


def dispatch_tables(ids, capacity, experts):
    tokens = ids.shape[1]
    lane = lax.broadcasted_iota(jnp.int32, (tokens, WIDE), 1)
    first = jnp.broadcast_to(ids[0:1].astype(F32), (tokens, tokens)).T.astype(jnp.int32)[:, :WIDE]
    second = jnp.broadcast_to(ids[1:2].astype(F32), (tokens, tokens)).T.astype(jnp.int32)[:, :WIDE]
    one = jnp.where(lane == first, 1.0, 0.0)
    two = jnp.where(lane == second, 1.0, 0.0)
    i, j = grid_of(tokens)
    before = jnp.where(i > j, 1.0, 0.0).astype(BF16)
    rank = dot(before, (one + two).astype(BF16)) + (lane * capacity).astype(F32)
    slot_one = jnp.sum(one * rank, -1, keepdims=True).astype(jnp.int32)
    slot_two = jnp.sum(two * rank, -1, keepdims=True).astype(jnp.int32)
    return slot_one, slot_two


def program_kernel(nz, nx, *refs):
    (
        q_in, k_in, v_in, beta_in, decay_in, ng_in, x_in, gain_in, ids_in, share_in,
        wg_in, wu_in, wd_in, mix_out, ffn_out,
        q_s, k_s, v_s, beta_s, decay_s, ng_s, x_s, gains, ids_s, share_s, wt, wd,
        rows_s, xs, xg, hg, ret, got, base_s, reach_s, total_s, state_in, state_out, mo_s, fo_s,
        load_sem, ready, disp_send, disp_recv, x_send, x_recv, hid_send, hid_recv,
        ret_send, ret_recv, g_send, g_recv, w_send, w_recv, s_send, s_recv,
    ) = refs
    grp, z, tp = lax.axis_index("grp"), lax.axis_index("ep"), lax.axis_index("tp")
    x, c = tp // 2, tp % 2
    partner = 2 * x + 1 - c
    tokens, feats = x_s.shape
    capacity = xs.shape[1]
    hid = wg_in.shape[0]
    groups = q_s.shape[0] // WIDE
    sources = nz // 2
    parity = z % 2
    mine = z // 2
    early = z < nz // 2
    first = z < nz // 4
    waits = []

    def remote(src, dst, send, recv, zz, tt):
        return pltpu.make_async_remote_copy(
            src_ref=src, dst_ref=dst, send_sem=send, recv_sem=recv,
            device_id=(grp, zz, tt), device_id_type=MESH,
        )

    def hop(k):
        return min(k, nz - k)

    places = [
        (x_in, x_s), (ids_in, ids_s), (beta_in, beta_s), (decay_in, decay_s), (k_in, k_s), (q_in, q_s),
        (v_in, v_s), (gain_in, gains.at[tp]), (share_in, share_s), (ng_in, ng_s),
        (wg_in, wt.at[pl.ds(pl.multiple_of(c * hid, hid), hid), :]),
        (wu_in, wt.at[pl.ds(pl.multiple_of((2 + c) * hid, hid), hid), :]),
        (wd_in, wd.at[c]),
    ]
    loads = [pltpu.make_async_copy(src, dst, load_sem.at[n]) for n, (src, dst) in enumerate(places)]
    for load in loads:
        load.start()

    barrier = pltpu.get_barrier_semaphore()
    for dt in sorted(range(1, 2 * nx), key=lambda k: -min(k, 2 * nx - k)):
        pl.semaphore_signal(
            barrier, inc=1, device_id=(grp, z, (tp + dt) % (2 * nx)), device_id_type=MESH
        )
    for k in range(1, nz):

        @pl.when(z + k < nz)
        def _():
            for core in range(2):
                pl.semaphore_signal(
                    barrier, inc=1, device_id=(grp, (z + k) % nz, 2 * x + core), device_id_type=MESH
                )

    def mixer_blocks():
        for g in range(groups):
            cut = slice(g * WIDE, (g + 1) * WIDE)
            rows_s[0, g : g + 1, :] = 1.0 / (1.0 + jnp.exp(-beta_s[:, cut]))
            rows_s[1, g : g + 1, :] = softplus(decay_s[:, cut])
        for g in range(groups, 8):
            rows_s[1, g : g + 1, :] = jnp.zeros((1, WIDE), F32)
        rows_s[2] = running_sums(rows_s[1])
        total = None
        for g in range(groups):
            cut = slice(g * WIDE, (g + 1) * WIDE)
            beta, cum = rows_s[0, g : g + 1, :], rows_s[2, g : g + 1, :]
            inverse = group_inverse(q_s[cut], k_s[cut], beta, cum)
            shift, transfer, base, reach = group_terms(q_s[cut], k_s[cut], v_s[cut], beta, cum, *inverse)
            if total is None:
                total = jnp.concatenate([shift, transfer], axis=1)
            else:
                through = dot_both(reach, total)
                base = base + through[:, :WIDE]
                reach = through[:, WIDE:]
                total = dot_both(transfer, total)
                total = jnp.concatenate([total[:, :WIDE] + shift, total[:, WIDE:]], axis=1)
            base_s[cut, :] = base
            reach_s[cut, :] = reach
        total_s[...] = total

    for n in range(2, 7):
        loads[n].wait()

    @pl.when(early)
    def _():
        mixer_blocks()

    pl.semaphore_wait(barrier, 2 * nx - 1 + 2 * z)

    for k in range(nz - 1, 0, -1):

        @pl.when(z >= k)
        def _():
            for core in range(2):
                pl.semaphore_signal(
                    ready.at[z], inc=1, device_id=(grp, (z + nz - k) % nz, 2 * x + core), device_id_type=MESH
                )

    loads[0].wait()
    loads[1].wait()
    slot_one, slot_two = dispatch_tables(ids_s[...], capacity, nz)
    slots = lax.broadcasted_iota(jnp.int32, (tokens, 2 * tokens), 1)
    chosen = jnp.where((slots == slot_one) | (slots == slot_two), 1.0, 0.0).astype(BF16)
    ordered = dot(chosen, x_s[...], TN).astype(BF16)
    for e in range(nz):
        xs[e] = ordered[e * capacity : (e + 1) * capacity]

    row_here = pl.ds(pl.multiple_of(mine * capacity, capacity), capacity)

    def rows_to(e):
        return remote(
            xs.at[e], xg.at[x, c, row_here, :], disp_send.at[e], disp_recv.at[mine, c], e, 2 * x + parity
        )

    for k in sorted(range(1, nz), key=lambda k: -hop(k)):

        @pl.when(z >= k)
        def _():
            rows_to((z + nz - k) % nz).start()

        waits.append((None, rows_to((z + k) % nz)))
    own = remote(xs.at[z], xg.at[x, c, row_here, :], disp_send.at[z], disp_recv.at[mine, c], z, partner)

    @pl.when(parity != c)
    def _():
        own.start()

    waits.append((parity != c, own))

    @pl.when(parity == c)
    def _():
        xg[x, c, row_here, :] = xs[z]

    loads[7].wait()
    for dt in range(1, 2 * nx):
        copy = remote(gains.at[tp], gains.at[tp], g_send.at[dt], g_recv.at[dt], z, (tp + dt) % (2 * nx))
        copy.start()
        waits.append((None, copy))
    to_partner = []
    for n, (src, dst) in enumerate(places[10:]):
        copy = remote(src, dst, w_send.at[n], w_recv.at[n], z, partner)
        copy.start()
        waits.append((None, copy))
        to_partner.append(copy)

    def ready_step(k, condition):
        e = (z + k) % nz

        @pl.when(jnp.logical_and(z + k < nz, condition))
        def _():
            pl.semaphore_wait(ready.at[e], 2)
            rows_to(e).start()

    cuts = [0]
    while cuts[-1] < sources:
        cuts.append(min(max(1, 2 * cuts[-1]), sources))
    pieces = len(cuts) - 1

    def span(n):
        return slice(cuts[n] * capacity, cuts[n + 1] * capacity)

    def features(chip, n, dx):
        part = xg.at[chip, :, pl.ds(cuts[n] * capacity, (cuts[n + 1] - cuts[n]) * capacity), :]
        return remote(part, part, x_send.at[dx, n], x_recv.at[dx, n], z, 2 * ((x + dx) % nx) + c)

    def hidden_of(chip, n, dx):
        part = hg.at[chip, pl.ds(cuts[n] * capacity, (cuts[n + 1] - cuts[n]) * capacity), :]
        return remote(part, part, hid_send.at[dx, n], hid_recv.at[dx, n], z, 2 * ((x + dx) % nx) + c)

    farthest = sorted(range(1, nx), key=lambda k: -min(k, nx - k))

    def gather_rows(n):
        for m in range(cuts[n], cuts[n + 1]):
            for core in range(2):
                landing = xg.at[x, core, pl.ds(m * capacity, capacity), :]
                arrival = remote(landing, landing, disp_send.at[0], disp_recv.at[m, core], z, partner)

                @pl.when(jnp.logical_or(2 * m + c != z, core != c))
                def _():
                    arrival.wait_recv()

        for dx in farthest:
            copy = features(x, n, dx)
            copy.start()
            waits.append((None, copy))

    def make_hidden(n):
        for dx in range(1, nx):
            features((x + nx - dx) % nx, n, dx).wait_recv()
        count = (cuts[n + 1] - cuts[n]) * capacity
        acc = jnp.zeros((count, 4 * hid), F32)
        squares = jnp.zeros((count, 1), F32)
        for member in range(2 * nx):
            part = xg[member // 2, member % 2, span(n), :].astype(F32)
            squares = squares + jnp.sum(part * part, -1, keepdims=True)
            scaled = (part * gains[member]).astype(BF16)
            acc = acc + dot(scaled, wt[:, member * feats : (member + 1) * feats], NT)
        scale = lax.rsqrt(squares / (feats * 2 * nx) + EPSILON)
        gate = acc[:, : 2 * hid] * scale
        up = acc[:, 2 * hid :] * scale
        hg[x, span(n), :] = (gate / (1.0 + jnp.exp(-gate)) * up).astype(BF16)
        for dx in farthest:
            copy = hidden_of(x, n, dx)
            copy.start()
            waits.append((None, copy))

    slot_here = pl.ds(pl.multiple_of(z * capacity, capacity), capacity)

    def give_back(n):
        for dx in range(1, nx):
            hidden_of((x + nx - dx) % nx, n, dx).wait_recv()
        hidden = jnp.concatenate([hg[chip, span(n), :] for chip in range(nx)], axis=1)
        for core in range(2):
            ret[core, span(n), :] = dot(hidden, wd[core]).astype(BF16)
        for m in range(cuts[n], cuts[n + 1]):
            target = 2 * m + c
            rows = pl.ds(m * capacity, capacity)
            for core in range(2):
                copy = remote(
                    ret.at[core, rows, :], got.at[slot_here, :], ret_send.at[m, core], ret_recv.at[z],
                    target, 2 * x + core,
                )
                away = jnp.logical_or(target != z, core != c)

                @pl.when(away)
                def _():
                    copy.start()

                waits.append((away, copy))

                @pl.when(jnp.logical_not(away))
                def _():
                    got[slot_here, :] = ret[core, rows, :]

    store_mix = pltpu.make_async_copy(mo_s, mix_out, load_sem.at[13])
    state = remote(state_out, state_in, s_send.at[0], s_recv.at[0], (z + 1) % nz, tp)

    def pass_state():
        @pl.when(z > 0)
        def _():
            state.wait_recv()

        @pl.when(z == 0)
        def _():
            state_in[...] = jnp.zeros_like(state_in)

        entering = state_in[...]

        @pl.when(z + 1 < nz)
        def _():
            leaving = dot_left(total_s[:, WIDE:], entering) + total_s[:, :WIDE]
            state_out[...] = leaving.astype(BF16)
            state.start()

        for g in range(groups):
            cut = slice(g * WIDE, (g + 1) * WIDE)
            raw = base_s[cut, :] + dot_left(reach_s[cut, :], entering)
            norm = lax.rsqrt(jnp.mean(raw * raw, -1, keepdims=True) + EPSILON)
            mo_s[cut, :] = (raw * norm * ng_s[...]).astype(BF16)
        store_mix.start()

    waits.append((z + 1 < nz, state))

    def weights_here():
        for load in loads[8:]:
            load.wait()
        for n in range(3):
            to_partner[n].wait_recv()
        for dt in range(1, 2 * nx):
            sender = (tp + 2 * nx - dt) % (2 * nx)
            remote(gains.at[sender], gains.at[sender], g_send.at[dt], g_recv.at[dt], z, sender).wait_recv()

    for k in range(1, nz):
        ready_step(k, first)
    after = jnp.logical_not(first)
    steps = iter(range(1, nz))

    def ready_steps(count):
        for k in [k for _, k in zip(range(count), steps)]:
            ready_step(k, after)

    ready_steps(1)
    gather_rows(0)
    ready_steps(2)
    if pieces > 1:
        gather_rows(1)
    weights_here()
    make_hidden(0)
    ready_steps(2)
    if pieces > 1:
        make_hidden(1)
    give_back(0)
    ready_steps(3)
    if pieces > 1:
        give_back(1)

    @pl.when(jnp.logical_not(early))
    def _():
        mixer_blocks()

    ready_steps(nz)
    for n in range(2, pieces):
        gather_rows(n)
    for n in range(2, pieces):
        make_hidden(n)
        give_back(n)
        if n == 2:

            @pl.when(early)
            def _():
                pass_state()

    if pieces < 3:

        @pl.when(early)
        def _():
            pass_state()

    @pl.when(jnp.logical_not(early))
    def _():
        pass_state()

    shares = share_s[...]
    first_share = jnp.broadcast_to(shares[0:1], (tokens, tokens)).T[:, :1]
    second_share = jnp.broadcast_to(shares[1:2], (tokens, tokens)).T[:, :1]
    weights = jnp.where(slots == slot_one, first_share, 0.0) + jnp.where(slots == slot_two, second_share, 0.0)
    for e in range(nz):
        landing = got.at[pl.ds(e * capacity, capacity), :]
        arrival = remote(landing, landing, disp_send.at[0], ret_recv.at[e], z, partner)

        @pl.when(jnp.logical_or(e != z, parity != c))
        def _():
            arrival.wait_recv()

    fo_s[...] = dot_left(weights, got[...]).astype(BF16)
    store_ffn = pltpu.make_async_copy(fo_s, ffn_out, load_sem.at[14])
    store_ffn.start()
    for condition, copy in waits:
        if condition is None:
            copy.wait_send()
        else:

            @pl.when(condition)
            def _():
                copy.wait_send()

    store_mix.wait()
    store_ffn.wait()


def body(nz, nx, mix_query, mix_keys, mix_values, beta_in, decay_in, norm_gain, ffn_input, ffn_gain,
         expert_ids, expert_share, w_gate, w_up, w_down):
    length, _, width = mix_query.shape
    tokens, feats = ffn_input.shape
    hid = w_gate.shape[2]
    full = w_gate.shape[1]
    capacity = 2 * tokens // nz
    rows = nz // 2 * capacity
    ff = w_down.shape[1]
    dma = pltpu.SemaphoreType.DMA
    vmem = pltpu.VMEM
    call = pl.pallas_call(
        functools.partial(program_kernel, nz, nx),
        out_shape=(
            jax.ShapeDtypeStruct((length, width), BF16),
            jax.ShapeDtypeStruct((tokens, feats), BF16),
        ),
        in_specs=[pl.BlockSpec(memory_space=pl.ANY)] * 13,
        out_specs=[pl.BlockSpec(memory_space=pl.ANY)] * 2,
        scratch_shapes=[
            vmem((length, width), BF16), vmem((length, width), BF16), vmem((length, width), BF16),
            vmem((1, length), F32), vmem((1, length), F32), vmem((1, width), F32),
            vmem((tokens, feats), BF16), vmem((2 * nx, 1, feats), F32),
            vmem((2, tokens), jnp.int32), vmem((2, tokens), F32),
            vmem((4 * hid, full), BF16), vmem((2, ff, feats), BF16),
            vmem((3, 8, width), F32),
            vmem((nz, capacity, feats), BF16),
            vmem((nx, 2, rows, feats), BF16),
            vmem((nx, rows, 2 * hid), BF16),
            vmem((2, rows, feats), BF16),
            vmem((2 * tokens, feats), BF16),
            vmem((length, width), F32), vmem((length, width), F32), vmem((width, 2 * width), F32),
            vmem((width, width), BF16), vmem((width, width), BF16),
            vmem((length, width), BF16), vmem((tokens, feats), BF16),
            dma((15,)), pltpu.SemaphoreType.REGULAR((nz,)), dma((nz,)), dma((nz // 2, 2)),
            dma((nx, 4)), dma((nx, 4)), dma((nx, 4)), dma((nx, 4)),
            dma((nz // 2, 2)), dma((nz,)),
            dma((2 * nx,)), dma((2 * nx,)), dma((3,)), dma((3,)), dma((1,)), dma((1,)),
        ],
        compiler_params=pltpu.CompilerParams(collective_id=0, has_side_effects=True),
    )
    mix, ffn = call(
        mix_query.reshape(length, width), mix_keys.reshape(length, width), mix_values.reshape(length, width),
        beta_in, decay_in, norm_gain.reshape(1, width), ffn_input, ffn_gain.reshape(1, feats),
        expert_ids.T, expert_share.T, w_gate[0].T, w_up[0].T, w_down[0],
    )
    return mix.reshape(length, 1, width), ffn


def solution(mesh):
    nz, nx = mesh.shape["ep"], mesh.shape["tp"] // 2
    in_specs = (
        P(("grp", "ep"), "tp", None), P(("grp", "ep"), "tp", None), P(("grp", "ep"), "tp", None),
        P("tp", ("grp", "ep")), P("tp", ("grp", "ep")), P(),
        P(("grp", "ep"), "tp"), P("tp"), P(("grp", "ep"), None), P(("grp", "ep"), None),
        P("ep", None, "tp"), P("ep", None, "tp"), P("ep", None, "tp"),
    )
    out_specs = (P(("grp", "ep"), "tp", None), P(("grp", "ep"), "tp"))
    return jax.shard_map(
        functools.partial(body, nz, nx), mesh=mesh, in_specs=in_specs, out_specs=out_specs, check_vma=False
    )
```

time: 96.7 us -> 101 us (1.044)
  the two profiles are of different devices: /device:TPU:80 before, /device:TPU:1856 now
where the time goes in v2:
time: 101 us
  Pallas kernels  98.1 us (97%)
  local copies, waits for them, and re-layouts  2.23 us (2%)
    pallas_call x1, Pallas kernels, body(): call(mix_query.reshape(length, width), mix_keys.reshape(length, width), m...  98.1 us
    unnamed x4, local copies, waits for them, and re-layouts  2.23 us

profile of v2, /device:TPU:1856, one launch (start us, length us, event | category | flops | bytes accessed | tf_op | source)
XLA Modules:
  0.0 101.0 jit_solution(8418590482617381017)
XLA Ops:
  0.6 98.1 %shard_map.140 = (bf16[512,128]{1,0:T(8,128)(2,1)}, bf16[128,256]{1,0:T(8,128)(2,1)}) custom-call(bf16[512,128]{1,0:T(8,128)(2,1)} %bitcast.18, bf16[512,128]{1,0:T(8,128)(2,1)} %bitcast.19, bf16[512,128]{1,0:T(8,128)(2,1)} %bitcast.20, f32[1,512]{1,0:T(1,128)} %refs_3_.1, f32[1,512]{1,0:T(1,128)} %refs_4_.1, f32[1,128]{1,0:T(1,128)} %bitcast.25, ...), custom_call_target="tpu_custom_call" | custom-call | tf_op jit(solution)/shard_map/pallas_call | solution.py:516
  98.8 0.0 copy-start
  98.8 1.6 %copy.17 = bf16[512,1,128]{2,0,1:T(8,128)(2,1)} copy(bf16[512,1,128]{2,0,1:T(8,128)(2,1)} %bitcast.21) | data formatting | bytes 262144
  100.4 0.0 copy-done
  100.4 0.6 copy.18
Async XLA Ops:
  98.8 1.6 %copy-start = (bf16[128,256]{1,0:T(8,128)(2,1)S(1)}, bf16[128,256]{1,0:T(8,128)(2,1)}, u32[]{:S(2)}) copy-start(bf16[128,256]{1,0:T(8,128)(2,1)} %get-tuple-element.9) | copy-start | bytes 196612

commit v3 on v2

v3 whole, which is shorter than its diff:
```python
import functools

import jax
import jax.numpy as jnp
from jax import lax
from jax.experimental import pallas as pl
from jax.experimental.pallas import tpu as pltpu
from jax.sharding import PartitionSpec as P

MESH = pl.DeviceIdType.MESH
EPSILON = 1e-06
BLOCK = 64
WIDE = 128
F32 = jnp.float32
BF16 = jnp.bfloat16

NN = ((1,), (0,))
NT = ((1,), (1,))
TN = ((0,), (0,))


def dot(a, b, dims=NN):
    return lax.dot_general(a, b, (dims, ((), ())), preferred_element_type=F32)


def halves(a):
    high = a.astype(BF16)
    return high, (a - high.astype(F32)).astype(BF16)


def dot_left(a, b, dims=NN):
    high, low = halves(a)
    return dot(high, b, dims) + dot(low, b, dims)


def dot_right(a, b, dims=NN):
    high, low = halves(b)
    return dot(a, high, dims) + dot(a, low, dims)


def dot_both(a, b, dims=NN):
    ah, al = halves(a)
    bh, bl = halves(b)
    return dot(ah, bh, dims) + (dot(ah, bl, dims) + dot(al, bh, dims))


def down_columns(row):
    return jnp.broadcast_to(row, (row.shape[1], row.shape[1])).T


def grid_of(n):
    return (
        lax.broadcasted_iota(jnp.int32, (n, n), 0),
        lax.broadcasted_iota(jnp.int32, (n, n), 1),
    )


def running_sums(rates):
    i, j = grid_of(WIDE)
    upper = jnp.where(i <= j, 1.0, 0.0).astype(BF16)
    high, rest = halves(rates)
    mid = (rates - high.astype(F32) - rest.astype(F32)).astype(BF16)
    return -(dot(high, upper) + (dot(rest, upper) + dot(mid, upper)))


def group_inverses(qs, ks, betas, cums):
    i, j = grid_of(WIDE)
    same = (i // BLOCK) == (j // BLOCK)
    each = range(len(qs))
    rqs, rks, scores, lowers = [], [], [], []
    for q, k, beta, cum in zip(qs, ks, betas, cums):
        qf, kf = q.astype(F32), k.astype(F32)
        rq = lax.rsqrt(jnp.sum(qf * qf, -1, keepdims=True) + EPSILON) * (WIDE**-0.5)
        rk = lax.rsqrt(jnp.sum(kf * kf, -1, keepdims=True) + EPSILON)
        rk_row = jnp.broadcast_to(rk, (WIDE, WIDE)).T
        spread = jnp.where(i >= j, down_columns(cum) - cum, 0.0)
        decay = jnp.exp(spread) * rk_row
        lowers.append(jnp.where(i > j, dot(k, k, NT) * rk * down_columns(beta) * decay, 0.0))
        scores.append(jnp.where(i >= j, dot(q, k, NT) * rq * decay, 0.0))
        rqs.append(rq)
        rks.append((rk, rk_row[:1]))
    powered = [jnp.where(same, -lowers[g], 0.0) for g in each]
    product = [jnp.where(i == j, 1.0, 0.0) + powered[g] for g in each]
    for _ in range(1, (BLOCK - 1).bit_length()):
        powered = [dot_both(powered[g], powered[g]) for g in each]
        product = [product[g] + dot_both(product[g], powered[g]) for g in each]
    crossed = [dot_both(jnp.where(same, 0.0, lowers[g]), product[g]) for g in each]
    inverses = [product[g] - dot_both(product[g], crossed[g]) for g in each]
    return [(inverses[g], scores[g], rqs[g], *rks[g]) for g in each]


def group_terms(q, k, v, beta, cum, inverse, scores, rq, rk, rk_row):
    i, j = grid_of(WIDE)
    cum_col = down_columns(cum)[:, :1]
    last = cum[:, WIDE - 1 :]
    update = dot_left(inverse * beta, v)
    correction = dot_left(inverse * (beta * jnp.exp(cum) * rk_row), k)
    both = jnp.concatenate([update, correction], axis=1)
    moved = dot_right(k, both * (rk * jnp.exp(last - cum_col)), TN)
    shift = moved[:, :WIDE]
    transfer = jnp.where(i == j, jnp.exp(last), 0.0) - moved[:, WIDE:]
    seen = dot_both(scores, both)
    base = seen[:, :WIDE]
    reach = q.astype(F32) * (rq * jnp.exp(cum_col)) - seen[:, WIDE:]
    return shift, transfer, base, reach


def softplus(x):
    return jnp.maximum(x, 0.0) + jnp.log1p(jnp.exp(-jnp.abs(x)))


def dispatch_tables(ids, capacity, experts):
    tokens = ids.shape[1]
    lane = lax.broadcasted_iota(jnp.int32, (tokens, WIDE), 1)
    first = jnp.broadcast_to(ids[0:1].astype(F32), (tokens, tokens)).T.astype(jnp.int32)[:, :WIDE]
    second = jnp.broadcast_to(ids[1:2].astype(F32), (tokens, tokens)).T.astype(jnp.int32)[:, :WIDE]
    one = jnp.where(lane == first, 1.0, 0.0)
    two = jnp.where(lane == second, 1.0, 0.0)
    i, j = grid_of(tokens)
    before = jnp.where(i > j, 1.0, 0.0).astype(BF16)
    rank = dot(before, (one + two).astype(BF16)) + (lane * capacity).astype(F32)
    slot_one = jnp.sum(one * rank, -1, keepdims=True).astype(jnp.int32)
    slot_two = jnp.sum(two * rank, -1, keepdims=True).astype(jnp.int32)
    return slot_one, slot_two


def program_kernel(nz, nx, *refs):
    (
        q_in, k_in, v_in, beta_in, decay_in, ng_in, x_in, gain_in, ids_in, share_in,
        wg_in, wu_in, wd_in, mix_out, ffn_out,
        q_s, k_s, v_s, beta_s, decay_s, ng_s, x_s, gains, ids_s, share_s, wt, wd,
        rows_s, xs, xg, hg, ret, got, base_s, reach_s, total_s, map_out, map_in, state_in, state_out, parts_s, mo_s, fo_s,
        load_sem, ready, disp_send, disp_recv, x_send, x_recv, hid_send, hid_recv,
        ret_send, ret_recv, g_send, g_recv, w_send, w_recv, s_send, s_recv, m_send, m_recv,
    ) = refs
    grp, z, tp = lax.axis_index("grp"), lax.axis_index("ep"), lax.axis_index("tp")
    x, c = tp // 2, tp % 2
    partner = 2 * x + 1 - c
    tokens, feats = x_s.shape
    capacity = xs.shape[1]
    hid = wg_in.shape[0]
    groups = q_s.shape[0] // WIDE
    sources = nz // 2
    parity = z % 2
    mine = z // 2
    first = z < nz // 4
    corner = jnp.logical_and(z == 0, tp == 0)
    usual = jnp.logical_not(corner)
    below = jnp.logical_and(z > 0, x == 0)
    beside = jnp.logical_and(z == 0, tp > 0)
    early = jnp.logical_and(z < nz // 2, usual)
    waits = []

    def remote(src, dst, send, recv, zz, tt):
        return pltpu.make_async_remote_copy(
            src_ref=src, dst_ref=dst, send_sem=send, recv_sem=recv,
            device_id=(grp, zz, tt), device_id_type=MESH,
        )

    def hop(k):
        return min(k, nz - k)

    barrier = pltpu.get_barrier_semaphore()

    def greet(sem, zz, tt):
        pl.semaphore_signal(sem, inc=1, device_id=(grp, zz, tt), device_id_type=MESH)

    around = sorted(range(1, 2 * nx), key=lambda k: -min(k, 2 * nx - k))

    @pl.when(below)
    def _():
        greet(barrier, 0, 0)

    @pl.when(usual)
    def _():
        for dt in around:
            greet(barrier, z, (tp + dt) % (2 * nx))

    for k in range(1, nz):

        @pl.when(jnp.logical_and(z + k < nz, usual))
        def _():
            for core in range(2):
                greet(barrier, (z + k) % nz, 2 * x + core)

    places = [
        (x_in, x_s), (ids_in, ids_s), (beta_in, beta_s), (decay_in, decay_s), (k_in, k_s), (q_in, q_s),
        (v_in, v_s), (gain_in, gains.at[tp]), (share_in, share_s), (ng_in, ng_s),
        (wg_in, wt.at[pl.ds(pl.multiple_of(c * hid, hid), hid), :]),
        (wu_in, wt.at[pl.ds(pl.multiple_of((2 + c) * hid, hid), hid), :]),
        (wd_in, wd.at[c]),
    ]
    loads = [pltpu.make_async_copy(src, dst, load_sem.at[n]) for n, (src, dst) in enumerate(places)]
    for load in loads:
        load.start()

    def mixer_blocks():
        for g in range(groups):
            cut = slice(g * WIDE, (g + 1) * WIDE)
            rows_s[0, g : g + 1, :] = 1.0 / (1.0 + jnp.exp(-beta_s[:, cut]))
            rows_s[1, g : g + 1, :] = softplus(decay_s[:, cut])
        for g in range(groups, 8):
            rows_s[1, g : g + 1, :] = jnp.zeros((1, WIDE), F32)
        rows_s[2] = running_sums(rows_s[1])
        cuts = [slice(g * WIDE, (g + 1) * WIDE) for g in range(groups)]
        qs, ks, vs = [q_s[cut] for cut in cuts], [k_s[cut] for cut in cuts], [v_s[cut] for cut in cuts]
        betas = [rows_s[0, g : g + 1, :] for g in range(groups)]
        cums = [rows_s[2, g : g + 1, :] for g in range(groups)]
        inverses = group_inverses(qs, ks, betas, cums)
        terms = [group_terms(qs[g], ks[g], vs[g], betas[g], cums[g], *inverses[g]) for g in range(groups)]
        total = None
        for cut, (shift, transfer, base, reach) in zip(cuts, terms):
            if total is None:
                total = jnp.concatenate([shift, transfer], axis=1)
            else:
                through = dot_both(reach, total)
                base = base + through[:, :WIDE]
                reach = through[:, WIDE:]
                total = dot_both(transfer, total)
                total = jnp.concatenate([total[:, :WIDE] + shift, total[:, WIDE:]], axis=1)
            base_s[cut, :] = base
            reach_s[cut, :] = reach
        total_s[...] = total
        map_out[...] = total.astype(BF16)

    loads[0].wait()
    loads[1].wait()
    slot_one, slot_two = dispatch_tables(ids_s[...], capacity, nz)
    slots = lax.broadcasted_iota(jnp.int32, (tokens, 2 * tokens), 1)
    chosen = jnp.where((slots == slot_one) | (slots == slot_two), 1.0, 0.0).astype(BF16)
    ordered = dot(chosen, x_s[...], TN).astype(BF16)
    for e in range(nz):
        xs[e] = ordered[e * capacity : (e + 1) * capacity]

    for n in range(2, 7):
        loads[n].wait()

    @pl.when(early)
    def _():
        mixer_blocks()

    missing = jnp.where(jnp.logical_or(below, beside), 1, 0)
    pl.semaphore_wait(barrier, 2 * nx - 1 + jnp.where(corner, 2 * (nz - 1), 2 * z - missing))

    for k in range(nz - 1, 0, -1):

        @pl.when(z >= k)
        def _():
            @pl.when(jnp.logical_or(z > k, x > 0))
            def _():
                greet(ready.at[z], (z + nz - k) % nz, 2 * x)

            greet(ready.at[z], (z + nz - k) % nz, 2 * x + 1)

    row_here = pl.ds(pl.multiple_of(mine * capacity, capacity), capacity)

    def rows_to(e):
        return remote(
            xs.at[e], xg.at[x, c, row_here, :], disp_send.at[e], disp_recv.at[mine, c], e, 2 * x + parity
        )

    for k in sorted(range(1, nz), key=lambda k: -hop(k)):
        to_corner = jnp.logical_and(z == k, jnp.logical_and(x == 0, parity == 0))

        @pl.when(jnp.logical_or(corner, jnp.logical_and(z >= k, jnp.logical_not(to_corner))))
        def _():
            rows_to((z + nz - k) % nz).start()

        waits.append((None, rows_to((z + k) % nz)))

    @pl.when(corner)
    def _():
        for dt in around:
            greet(ready.at[0], z, (tp + dt) % (2 * nx))
        for k in range(1, nz):
            for core in range(2):
                greet(ready.at[0], (z + k) % nz, 2 * x + core)

    own = remote(xs.at[z], xg.at[x, c, row_here, :], disp_send.at[z], disp_recv.at[mine, c], z, partner)
    own_away = jnp.logical_and(beside, tp == 1)

    @pl.when(jnp.logical_and(parity != c, jnp.logical_not(own_away)))
    def _():
        own.start()

    waits.append((parity != c, own))

    @pl.when(parity == c)
    def _():
        xg[x, c, row_here, :] = xs[z]

    loads[7].wait()

    def gains_to(dt):
        return remote(gains.at[tp], gains.at[tp], g_send.at[dt], g_recv.at[dt], z, (tp + dt) % (2 * nx))

    for dt in range(1, 2 * nx):

        @pl.when(jnp.logical_or(z > 0, (tp + dt) % (2 * nx) > 0))
        def _():
            gains_to(dt).start()

        waits.append((None, gains_to(dt)))
    to_partner = [remote(src, dst, w_send.at[n], w_recv.at[n], z, partner) for n, (src, dst) in enumerate(places[10:])]

    @pl.when(jnp.logical_not(own_away))
    def _():
        for copy in to_partner:
            copy.start()

    for copy in to_partner:
        waits.append((None, copy))

    @pl.when(corner)
    def _():
        mixer_blocks()

    def ready_step(k, condition):
        e = (z + k) % nz

        @pl.when(jnp.logical_and(z + k < nz, condition))
        def _():
            pl.semaphore_wait(ready.at[e], 2)
            rows_to(e).start()

    def block(ref, lead, begin, end):
        return ref.at[lead, pl.ds(begin * capacity, (end - begin) * capacity), :]

    def features(chip, begin, end, sem, dx):
        part = xg.at[chip, :, pl.ds(begin * capacity, (end - begin) * capacity), :]
        return remote(part, part, x_send.at[dx, sem], x_recv.at[dx, sem], z, 2 * ((x + dx) % nx) + c)

    def hidden_of(chip, begin, end, sem, dx):
        part = block(hg, chip, begin, end)
        return remote(part, part, hid_send.at[dx, sem], hid_recv.at[dx, sem], z, 2 * ((x + dx) % nx) + c)

    farthest = sorted(range(1, nx), key=lambda k: -min(k, nx - k))
    branch = [None]
    gathered = []

    def started(make, *at):
        make(*at).start()
        waits.append((branch[0], functools.partial(make, *at)))

    def meet_corner(spans=()):
        @pl.when(jnp.logical_or(below, beside))
        def _():
            pl.semaphore_wait(ready.at[0], 1)

            @pl.when(jnp.logical_and(below, parity == 0))
            def _():
                rows_to(0).start()

        if spans:

            @pl.when(beside)
            def _():
                gains_to(2 * nx - tp).start()

                @pl.when(tp == 1)
                def _():
                    own.start()
                    for copy in to_partner:
                        copy.start()

                @pl.when(c == 0)
                def _():
                    for n, (b, e) in enumerate(spans):
                        features(x, b, e, n, nx - x).start()

    def gather_rows(begin, end, sem, skip_corner=False, condition=None):
        def go():
            for m in range(begin, end):
                for core in range(2):
                    landing = xg.at[x, core, pl.ds(m * capacity, capacity), :]
                    arrival = remote(landing, landing, disp_send.at[0], disp_recv.at[m, core], z, partner)

                    @pl.when(jnp.logical_or(2 * m + c != z, core != c))
                    def _():
                        arrival.wait_recv()

            for dx in farthest:
                skipped = jnp.logical_and(jnp.logical_and(z == 0, c == 0), (x + dx) % nx == 0)

                @pl.when(jnp.logical_not(jnp.logical_and(skipped, skip_corner)))
                def _():
                    features(x, begin, end, sem, dx).start()

        if condition is None:
            go()
        else:
            pl.when(condition)(go)
        if (begin, end, sem, branch[0] is first) not in gathered:
            gathered.append((begin, end, sem, branch[0] is first))
            for dx in farthest:
                waits.append((branch[0], functools.partial(features, x, begin, end, sem, dx)))

    def make_hidden(begin, end, parts, sem):
        for first_row, last_row, part_sem in parts:
            for dx in range(1, nx):
                features((x + nx - dx) % nx, first_row, last_row, part_sem, dx).wait_recv()
        rows = slice(begin * capacity, end * capacity)
        acc = jnp.zeros(((end - begin) * capacity, 4 * hid), F32)
        squares = jnp.zeros(((end - begin) * capacity, 1), F32)
        for member in range(2 * nx):
            part = xg[member // 2, member % 2, rows, :].astype(F32)
            squares = squares + jnp.sum(part * part, -1, keepdims=True)
            scaled = (part * gains[member]).astype(BF16)
            acc = acc + dot(scaled, wt[:, member * feats : (member + 1) * feats], NT)
        scale = lax.rsqrt(squares / (feats * 2 * nx) + EPSILON)
        gate = acc[:, : 2 * hid] * scale
        up = acc[:, 2 * hid :] * scale
        hg[x, rows, :] = (gate / (1.0 + jnp.exp(-gate)) * up).astype(BF16)
        for dx in farthest:
            started(hidden_of, x, begin, end, sem, dx)

    slot_here = pl.ds(pl.multiple_of(z * capacity, capacity), capacity)

    def result(m, core):
        return remote(
            ret.at[core, pl.ds(m * capacity, capacity), :], got.at[slot_here, :],
            ret_send.at[m, core], ret_recv.at[z], 2 * m + c, 2 * x + core,
        )

    def away(m, core):
        return jnp.logical_or(2 * m + c != z, core != c)

    def give_back(begin, end, sem):
        for dx in range(1, nx):
            hidden_of((x + nx - dx) % nx, begin, end, sem, dx).wait_recv()
        rows = slice(begin * capacity, end * capacity)
        hidden = jnp.concatenate([hg[chip, rows, :] for chip in range(nx)], axis=1)
        for core in range(2):
            ret[core, rows, :] = dot(hidden, wd[core]).astype(BF16)
        for m in range(begin, end):
            for core in range(2):

                @pl.when(away(m, core))
                def _():
                    result(m, core).start()

                @pl.when(jnp.logical_not(away(m, core)))
                def _():
                    got[slot_here, :] = ret[core, m * capacity : (m + 1) * capacity, :]

    for m in range(sources):
        for core in range(2):
            waits.append((away(m, core), result(m, core)))

    store_mix = pltpu.make_async_copy(mo_s, mix_out, load_sem.at[13])
    odd = z % 2 == 1
    send_map = jnp.logical_and(jnp.logical_not(odd), z + 1 < nz)
    own_map = remote(map_out, map_in, m_send.at[0], m_recv.at[0], (z + 1) % nz, tp)
    state_near = remote(state_out, state_in, s_send.at[0], s_recv.at[0], (z + 1) % nz, tp)
    state_far = remote(state_out, state_in, s_send.at[1], s_recv.at[0], (z + 2) % nz, tp)
    waits.append((send_map, own_map))
    waits.append((jnp.logical_and(odd, z + 1 < nz), state_near))
    waits.append((jnp.logical_and(odd, z + 2 < nz), state_far))

    def pass_map(condition):
        @pl.when(jnp.logical_and(condition, send_map))
        def _():
            own_map.start()

    def pass_state():
        @pl.when(z > 1)
        def _():
            state_near.wait_recv()

        @pl.when(z <= 1)
        def _():
            state_in[...] = jnp.zeros_like(state_in)

        @pl.when(odd)
        def _():
            own_map.wait_recv()
            before = map_in[...]
            entering = dot_right(before[:, WIDE:], state_in[...].astype(F32)) + before[:, :WIDE].astype(F32)
            leaving = dot_both(total_s[:, WIDE:], entering) + total_s[:, :WIDE]
            state_out[...] = leaving.astype(BF16)
            high, low = halves(entering)
            parts_s[0] = high
            parts_s[1] = low

            @pl.when(z + 2 < nz)
            def _():
                state_far.start()

            @pl.when(z + 1 < nz)
            def _():
                state_near.start()

        @pl.when(jnp.logical_not(odd))
        def _():
            parts_s[0] = state_in[...]
            parts_s[1] = jnp.zeros_like(state_in)

        for g in range(groups):
            cut = slice(g * WIDE, (g + 1) * WIDE)
            high, low = halves(reach_s[cut, :])
            across = dot(high, parts_s[1]) + dot(low, parts_s[0])
            raw = base_s[cut, :] + (dot(high, parts_s[0]) + across)
            norm = lax.rsqrt(jnp.mean(raw * raw, -1, keepdims=True) + EPSILON)
            mo_s[cut, :] = (raw * norm * ng_s[...]).astype(BF16)
        store_mix.start()

    def weights_here():
        for load in loads[8:]:
            load.wait()
        for n in range(3):
            to_partner[n].wait_recv()
        for dt in range(1, 2 * nx):
            sender = (tp + 2 * nx - dt) % (2 * nx)
            remote(gains.at[sender], gains.at[sender], g_send.at[dt], g_recv.at[dt], z, sender).wait_recv()

    def marks(*fractions):
        found = [0]
        for part, whole in fractions:
            found.append(max(found[-1], sources * part // whole))
        found.append(sources)
        return [(b, e) for b, e in zip(found[:-1], found[1:]) if e > b]

    branch[0] = first

    @pl.when(first)
    def _():
        steps = iter(range(1, nz))

        def ready_steps(count):
            for k in [k for _, k in zip(range(count), steps)]:
                ready_step(k, usual)

        spans = marks((1, 4), (2, 4), (3, 4), (7, 8))
        last_span = len(spans) - 1
        ready_steps(1)
        pass_map(first)
        ready_steps(nz // 4 - 1)
        waiting = jnp.logical_and(below, c == 0)
        before, later = list(enumerate(spans[:-1]))[:2], list(enumerate(spans[:-1]))[2:]
        for n, (b, e) in before:
            gather_rows(b, e, n, True, jnp.logical_not(waiting) if n == 0 else None)
            ready_steps(nz // 4 if n == 0 else nz // 8)
        meet_corner(spans[: len(before)])
        gather_rows(*spans[0], 0, False, waiting)
        ready_steps(nz // 8)
        for n, (b, e) in later:
            gather_rows(b, e, n)
            ready_steps(1)
        ready_steps(nz)
        weights_here()
        bulk = spans[last_span][0]
        half = spans[min(2, last_span)][0]
        inner = [(b, e, n) for n, (b, e) in enumerate(spans)]
        parts = [(b, e) for b, e in ((0, half), (half, bulk), (bulk, sources)) if e > b]
        given = 0
        for n, (b, e) in enumerate(parts):
            if n == len(parts) - 1 and n > 1:
                give_back(*parts[0], 0)
                given = 1
            make_hidden(b, e, [p for p in inner if b <= p[0] < e], n)
            if n == 0:
                gather_rows(bulk, sources, last_span)
        for n in range(given, len(parts)):
            give_back(*parts[n], n)

    after = jnp.logical_not(first)
    branch[0] = after

    @pl.when(after)
    def _():
        steps = iter(range(1, nz))

        def ready_steps(count):
            for k in [k for _, k in zip(range(count), steps)]:
                ready_step(k, usual)

        spans = marks((1, 8), (2, 8), (4, 8), (6, 8))
        count = len(spans)

        def gather(n):
            if n < count:
                gather_rows(*spans[n], n)

        def hide(n):
            if n < count:
                make_hidden(*spans[n], [(*spans[n], n)], n)

        def give(n):
            if n < count:
                give_back(*spans[n], n)

        ready_steps(1)
        pass_map(early)
        meet_corner()
        gather(0)
        ready_steps(2)
        gather(1)
        ready_steps(nz)
        weights_here()
        hide(0)
        hide(1)
        gather(2)
        give(0)
        give(1)
        hide(2)
        gather(3)
        give(2)
        gather(4)
        for n in range(3, count):
            hide(n)
        for n in range(3, count):
            give(n)

    @pl.when(z >= nz // 2)
    def _():
        mixer_blocks()

    pass_map(z >= nz // 2)
    pass_state()

    shares = share_s[...]
    first_share = jnp.broadcast_to(shares[0:1], (tokens, tokens)).T[:, :1]
    second_share = jnp.broadcast_to(shares[1:2], (tokens, tokens)).T[:, :1]
    weights = jnp.where(slots == slot_one, first_share, 0.0) + jnp.where(slots == slot_two, second_share, 0.0)
    for e in range(nz):
        landing = got.at[pl.ds(e * capacity, capacity), :]
        arrival = remote(landing, landing, disp_send.at[0], ret_recv.at[e], z, partner)

        @pl.when(jnp.logical_or(e != z, parity != c))
        def _():
            arrival.wait_recv()

    fo_s[...] = dot_left(weights, got[...]).astype(BF16)
    store_ffn = pltpu.make_async_copy(fo_s, ffn_out, load_sem.at[14])
    store_ffn.start()
    for condition, copy in waits:

        def settle():
            (copy() if callable(copy) else copy).wait_send()

        if condition is None:
            settle()
        else:
            pl.when(condition)(settle)

    store_mix.wait()
    store_ffn.wait()


def body(nz, nx, mix_query, mix_keys, mix_values, beta_in, decay_in, norm_gain, ffn_input, ffn_gain,
         expert_ids, expert_share, w_gate, w_up, w_down):
    length, _, width = mix_query.shape
    tokens, feats = ffn_input.shape
    hid = w_gate.shape[2]
    full = w_gate.shape[1]
    capacity = 2 * tokens // nz
    rows = nz // 2 * capacity
    ff = w_down.shape[1]
    dma = pltpu.SemaphoreType.DMA
    vmem = pltpu.VMEM
    call = pl.pallas_call(
        functools.partial(program_kernel, nz, nx),
        out_shape=(
            jax.ShapeDtypeStruct((length, width), BF16),
            jax.ShapeDtypeStruct((tokens, feats), BF16),
        ),
        in_specs=[pl.BlockSpec(memory_space=pl.ANY)] * 13,
        out_specs=[pl.BlockSpec(memory_space=pl.ANY)] * 2,
        scratch_shapes=[
            vmem((length, width), BF16), vmem((length, width), BF16), vmem((length, width), BF16),
            vmem((1, length), F32), vmem((1, length), F32), vmem((1, width), F32),
            vmem((tokens, feats), BF16), vmem((2 * nx, 1, feats), F32),
            vmem((2, tokens), jnp.int32), vmem((2, tokens), F32),
            vmem((4 * hid, full), BF16), vmem((2, ff, feats), BF16),
            vmem((3, 8, width), F32),
            vmem((nz, capacity, feats), BF16),
            vmem((nx, 2, rows, feats), BF16),
            vmem((nx, rows, 2 * hid), BF16),
            vmem((2, rows, feats), BF16),
            vmem((2 * tokens, feats), BF16),
            vmem((length, width), F32), vmem((length, width), F32), vmem((width, 2 * width), F32),
            vmem((width, 2 * width), BF16), vmem((width, 2 * width), BF16),
            vmem((width, width), BF16), vmem((width, width), BF16), vmem((2, width, width), BF16),
            vmem((length, width), BF16), vmem((tokens, feats), BF16),
            dma((15,)), pltpu.SemaphoreType.REGULAR((nz,)), dma((nz,)), dma((nz // 2, 2)),
            dma((nx, 5)), dma((nx, 5)), dma((nx, 5)), dma((nx, 5)),
            dma((nz // 2, 2)), dma((nz,)),
            dma((2 * nx,)), dma((2 * nx,)), dma((3,)), dma((3,)), dma((2,)), dma((1,)), dma((1,)), dma((1,)),
        ],
        compiler_params=pltpu.CompilerParams(collective_id=0, has_side_effects=True),
    )
    mix, ffn = call(
        mix_query.reshape(length, width), mix_keys.reshape(length, width), mix_values.reshape(length, width),
        beta_in, decay_in, norm_gain.reshape(1, width), ffn_input, ffn_gain.reshape(1, feats),
        expert_ids.T, expert_share.T, w_gate[0].T, w_up[0].T, w_down[0],
    )
    return mix.reshape(length, 1, width), ffn


def solution(mesh):
    nz, nx = mesh.shape["ep"], mesh.shape["tp"] // 2
    in_specs = (
        P(("grp", "ep"), "tp", None), P(("grp", "ep"), "tp", None), P(("grp", "ep"), "tp", None),
        P("tp", ("grp", "ep")), P("tp", ("grp", "ep")), P(),
        P(("grp", "ep"), "tp"), P("tp"), P(("grp", "ep"), None), P(("grp", "ep"), None),
        P("ep", None, "tp"), P("ep", None, "tp"), P("ep", None, "tp"),
    )
    out_specs = (P(("grp", "ep"), "tp", None), P(("grp", "ep"), "tp"))
    return jax.shard_map(
        functools.partial(body, nz, nx), mesh=mesh, in_specs=in_specs, out_specs=out_specs, check_vma=False
    )
```

time: 101 us -> 81.9 us (0.81)
  the two profiles are of different devices: /device:TPU:1856 before, /device:TPU:80 now
where the time goes in v3:
time: 81.9 us; the launch traced here: 81.8 us
  Pallas kernels  78.9 us (96%)
  local copies, waits for them, and re-layouts  2.23 us (3%)
    pallas_call x1, Pallas kernels, body(): call(mix_query.reshape(length, width), mix_keys.reshape(length, width), m...  78.9 us
    unnamed x4, local copies, waits for them, and re-layouts  2.23 us

profile of v3, /device:TPU:80, one launch (start us, length us, event | category | flops | bytes accessed | tf_op | source)
XLA Modules:
  0.0 81.8 jit_solution(9928107352884427616)
XLA Ops:
  0.6 78.9 %shard_map.140 = (bf16[512,128]{1,0:T(8,128)(2,1)}, bf16[128,256]{1,0:T(8,128)(2,1)}) custom-call(bf16[512,128]{1,0:T(8,128)(2,1)} %bitcast.18, bf16[512,128]{1,0:T(8,128)(2,1)} %bitcast.19, bf16[512,128]{1,0:T(8,128)(2,1)} %bitcast.20, f32[1,512]{1,0:T(1,128)} %refs_3_.1, f32[1,512]{1,0:T(1,128)} %refs_4_.1, f32[1,128]{1,0:T(1,128)} %bitcast.25, ...), custom_call_target="tpu_custom_call" | custom-call | tf_op jit(solution)/shard_map/pallas_call | solution.py:692
  79.5 0.0 copy-start
  79.5 1.6 %copy.17 = bf16[512,1,128]{2,0,1:T(8,128)(2,1)} copy(bf16[512,1,128]{2,0,1:T(8,128)(2,1)} %bitcast.21) | data formatting | bytes 262144
  81.1 0.0 copy-done
  81.1 0.6 copy.18
Async XLA Ops:
  79.5 1.6 %copy-start = (bf16[128,256]{1,0:T(8,128)(2,1)S(1)}, bf16[128,256]{1,0:T(8,128)(2,1)}, u32[]{:S(2)}) copy-start(bf16[128,256]{1,0:T(8,128)(2,1)} %get-tuple-element.9) | copy-start | bytes 196612

commit v4 on v3

--- a/solution.py
+++ b/solution.py
@@ -129,8 +129,8 @@
         q_in, k_in, v_in, beta_in, decay_in, ng_in, x_in, gain_in, ids_in, share_in,
         wg_in, wu_in, wd_in, mix_out, ffn_out,
         q_s, k_s, v_s, beta_s, decay_s, ng_s, x_s, gains, ids_s, share_s, wt, wd,
-        rows_s, xs, xg, hg, ret, got, base_s, reach_s, total_s, map_out, map_in, state_in, state_out, parts_s, mo_s, fo_s,
-        load_sem, ready, disp_send, disp_recv, x_send, x_recv, hid_send, hid_recv,
+        rows_s, xs, xg, alt, hg, ret, got, base_s, reach_s, total_s, map_out, map_in, state_in, state_out, parts_s,
+        load_sem, ready, disp_send, disp_recv, alt_send, alt_recv, x_send, x_recv, hid_send, hid_recv,
         ret_send, ret_recv, g_send, g_recv, w_send, w_recv, s_send, s_recv, m_send, m_recv,
     ) = refs
     grp, z, tp = lax.axis_index("grp"), lax.axis_index("ep"), lax.axis_index("tp")
@@ -141,13 +141,15 @@
     hid = wg_in.shape[0]
     groups = q_s.shape[0] // WIDE
     sources = nz // 2
-    parity = z % 2
+    home = 1 - z % 2
     mine = z // 2
     first = z < nz // 4
     corner = jnp.logical_and(z == 0, tp == 0)
     usual = jnp.logical_not(corner)
     below = jnp.logical_and(z > 0, x == 0)
     beside = jnp.logical_and(z == 0, tp > 0)
+    proxy = jnp.logical_and(z == 0, tp == 1)
+    first_usual = jnp.logical_and(first, usual)
     early = jnp.logical_and(z < nz // 2, usual)
     waits = []
 
@@ -256,43 +258,48 @@
 
     def rows_to(e):
         return remote(
-            xs.at[e], xg.at[x, c, row_here, :], disp_send.at[e], disp_recv.at[mine, c], e, 2 * x + parity
+            xs.at[e], xg.at[x, c, row_here, :], disp_send.at[0], disp_recv.at[mine, c], e, 2 * x + home
         )
 
+    rows_aside = remote(xs.at[0], alt.at[c, row_here, :], disp_send.at[0], alt_recv.at[mine, c], 0, 1)
+
     for k in sorted(range(1, nz), key=lambda k: -hop(k)):
-        to_corner = jnp.logical_and(z == k, jnp.logical_and(x == 0, parity == 0))
-
-        @pl.when(jnp.logical_or(corner, jnp.logical_and(z >= k, jnp.logical_not(to_corner))))
+        aside = jnp.logical_and(z == k, jnp.logical_and(x == 0, home == 0))
+
+        @pl.when(jnp.logical_or(corner, jnp.logical_and(z >= k, jnp.logical_not(aside))))
         def _():
             rows_to((z + nz - k) % nz).start()
 
-        waits.append((None, rows_to((z + k) % nz)))
+        @pl.when(aside)
+        def _():
+            rows_aside.start()
 
     @pl.when(corner)
     def _():
         for dt in around:
             greet(ready.at[0], z, (tp + dt) % (2 * nx))
-        for k in range(1, nz):
+        for k in sorted(range(1, nz), key=lambda k: -hop(k)):
             for core in range(2):
                 greet(ready.at[0], (z + k) % nz, 2 * x + core)
 
-    own = remote(xs.at[z], xg.at[x, c, row_here, :], disp_send.at[z], disp_recv.at[mine, c], z, partner)
-    own_away = jnp.logical_and(beside, tp == 1)
-
-    @pl.when(jnp.logical_and(parity != c, jnp.logical_not(own_away)))
+    all_rows = xs.at[pl.ds(0, nz - 1)]
+    waits.append((None, remote(all_rows, all_rows, disp_send.at[0], disp_recv.at[0, 0], z, partner)))
+    own = remote(xs.at[z], xg.at[x, c, row_here, :], disp_send.at[1], disp_recv.at[mine, c], z, partner)
+
+    @pl.when(home != c)
     def _():
         own.start()
 
-    waits.append((parity != c, own))
-
-    @pl.when(parity == c)
+    waits.append((home != c, own))
+
+    @pl.when(home == c)
     def _():
         xg[x, c, row_here, :] = xs[z]
 
     loads[7].wait()
 
     def gains_to(dt):
-        return remote(gains.at[tp], gains.at[tp], g_send.at[dt], g_recv.at[dt], z, (tp + dt) % (2 * nx))
+        return remote(gains.at[tp], gains.at[tp], g_send.at[0], g_recv.at[0], z, (tp + dt) % (2 * nx))
 
     for dt in range(1, 2 * nx):
 
@@ -300,10 +307,12 @@
         def _():
             gains_to(dt).start()
 
-        waits.append((None, gains_to(dt)))
+    all_gains = gains.at[pl.ds(0, 2 * nx - 1)]
+    gains_of_all = remote(all_gains, all_gains, g_send.at[0], g_recv.at[0], z, partner)
+    waits.append((None, gains_of_all))
     to_partner = [remote(src, dst, w_send.at[n], w_recv.at[n], z, partner) for n, (src, dst) in enumerate(places[10:])]
 
-    @pl.when(jnp.logical_not(own_away))
+    @pl.when(jnp.logical_not(proxy))
     def _():
         for copy in to_partner:
             copy.start()
@@ -323,33 +332,56 @@
             pl.semaphore_wait(ready.at[e], 2)
             rows_to(e).start()
 
+    def away(m, core):
+        return jnp.logical_or(2 * m + 1 - c != z, core != c)
+
     def block(ref, lead, begin, end):
         return ref.at[lead, pl.ds(begin * capacity, (end - begin) * capacity), :]
 
     def features(chip, begin, end, sem, dx):
         part = xg.at[chip, :, pl.ds(begin * capacity, (end - begin) * capacity), :]
-        return remote(part, part, x_send.at[dx, sem], x_recv.at[dx, sem], z, 2 * ((x + dx) % nx) + c)
+        return remote(part, part, x_send.at[sem], x_recv.at[sem], z, 2 * ((x + dx) % nx) + c)
+
+    def all_features(begin, end, sem, count):
+        part = xg.at[pl.ds(0, count), :, pl.ds(begin * capacity, (end - begin) * capacity), :]
+        return remote(part, part, x_send.at[sem], x_recv.at[sem], z, partner)
+
+    def all_hidden(begin, end, sem):
+        part = hg.at[pl.ds(0, nx - 1), pl.ds(begin * capacity, (end - begin) * capacity), :]
+        return remote(part, part, hid_send.at[sem], hid_recv.at[sem], z, partner)
 
     def hidden_of(chip, begin, end, sem, dx):
         part = block(hg, chip, begin, end)
-        return remote(part, part, hid_send.at[dx, sem], hid_recv.at[dx, sem], z, 2 * ((x + dx) % nx) + c)
+        return remote(part, part, hid_send.at[sem], hid_recv.at[sem], z, 2 * ((x + dx) % nx) + c)
 
     farthest = sorted(range(1, nx), key=lambda k: -min(k, nx - k))
     branch = [None]
     gathered = []
 
-    def started(make, *at):
-        make(*at).start()
-        waits.append((branch[0], functools.partial(make, *at)))
+    def set_aside(begin, end, sem, dx):
+        rows = pl.ds(begin * capacity, (end - begin) * capacity)
+        return remote(alt.at[:, rows, :], xg.at[0, :, rows, :], alt_send.at[sem], x_recv.at[sem], z, 2 * dx)
+
+    def gather_aside(begin, end, sem, skip_corner):
+        @pl.when(proxy)
+        def _():
+            for m in range(begin, end):
+                for core in range(2):
+                    landing = alt.at[core, pl.ds(m * capacity, capacity), :]
+                    remote(landing, landing, disp_send.at[0], alt_recv.at[m, core], z, partner).wait_recv()
+            for dx in farthest + ([] if skip_corner else [0]):
+                set_aside(begin, end, sem, dx).start()
+
+        def gone():
+            part = xg.at[:, :, pl.ds(begin * capacity, (end - begin) * capacity), :]
+            return remote(part, part, alt_send.at[sem], x_recv.at[sem], z, partner)
+
+        waits.append((proxy, gone))
 
     def meet_corner(spans=()):
         @pl.when(jnp.logical_or(below, beside))
         def _():
             pl.semaphore_wait(ready.at[0], 1)
-
-            @pl.when(jnp.logical_and(below, parity == 0))
-            def _():
-                rows_to(0).start()
 
         if spans:
 
@@ -359,9 +391,10 @@
 
                 @pl.when(tp == 1)
                 def _():
-                    own.start()
                     for copy in to_partner:
                         copy.start()
+                    for n, (b, e) in enumerate(spans):
+                        set_aside(b, e, n, 0).start()
 
                 @pl.when(c == 0)
                 def _():
@@ -375,7 +408,7 @@
                     landing = xg.at[x, core, pl.ds(m * capacity, capacity), :]
                     arrival = remote(landing, landing, disp_send.at[0], disp_recv.at[m, core], z, partner)
 
-                    @pl.when(jnp.logical_or(2 * m + c != z, core != c))
+                    @pl.when(away(m, core))
                     def _():
                         arrival.wait_recv()
 
@@ -386,19 +419,23 @@
                 def _():
                     features(x, begin, end, sem, dx).start()
 
-        if condition is None:
-            go()
-        else:
-            pl.when(condition)(go)
-        if (begin, end, sem, branch[0] is first) not in gathered:
-            gathered.append((begin, end, sem, branch[0] is first))
-            for dx in farthest:
-                waits.append((branch[0], functools.partial(features, x, begin, end, sem, dx)))
+        pl.when(usual if condition is None else jnp.logical_and(usual, condition))(go)
+        made = (begin, end, sem, branch[0] is first)
+        if made not in gathered:
+            gathered.append(made)
+            sent = first_usual if branch[0] is first else branch[0]
+            waits.append((sent, functools.partial(all_features, begin, end, sem, nx - 1)))
 
     def make_hidden(begin, end, parts, sem):
         for first_row, last_row, part_sem in parts:
-            for dx in range(1, nx):
-                features((x + nx - dx) % nx, first_row, last_row, part_sem, dx).wait_recv()
+            @pl.when(corner)
+            def _():
+                all_features(first_row, last_row, part_sem, nx).wait_recv()
+
+            @pl.when(usual)
+            def _():
+                all_features(first_row, last_row, part_sem, nx - 1).wait_recv()
+
         rows = slice(begin * capacity, end * capacity)
         acc = jnp.zeros(((end - begin) * capacity, 4 * hid), F32)
         squares = jnp.zeros(((end - begin) * capacity, 1), F32)
@@ -412,22 +449,20 @@
         up = acc[:, 2 * hid :] * scale
         hg[x, rows, :] = (gate / (1.0 + jnp.exp(-gate)) * up).astype(BF16)
         for dx in farthest:
-            started(hidden_of, x, begin, end, sem, dx)
-
+            hidden_of(x, begin, end, sem, dx).start()
+        waits.append((branch[0], functools.partial(all_hidden, begin, end, sem)))
+
+    rows_all = sources * capacity
     slot_here = pl.ds(pl.multiple_of(z * capacity, capacity), capacity)
 
     def result(m, core):
         return remote(
             ret.at[core, pl.ds(m * capacity, capacity), :], got.at[slot_here, :],
-            ret_send.at[m, core], ret_recv.at[z], 2 * m + c, 2 * x + core,
+            ret_send.at[0], ret_recv.at[0], 2 * m + 1 - c, 2 * x + core,
         )
 
-    def away(m, core):
-        return jnp.logical_or(2 * m + c != z, core != c)
-
     def give_back(begin, end, sem):
-        for dx in range(1, nx):
-            hidden_of((x + nx - dx) % nx, begin, end, sem, dx).wait_recv()
+        all_hidden(begin, end, sem).wait_recv()
         rows = slice(begin * capacity, end * capacity)
         hidden = jnp.concatenate([hg[chip, rows, :] for chip in range(nx)], axis=1)
         for core in range(2):
@@ -443,11 +478,12 @@
                 def _():
                     got[slot_here, :] = ret[core, m * capacity : (m + 1) * capacity, :]
 
-    for m in range(sources):
-        for core in range(2):
-            waits.append((away(m, core), result(m, core)))
-
-    store_mix = pltpu.make_async_copy(mo_s, mix_out, load_sem.at[13])
+    at_home = home == c
+    results_gone = ret.at[:, pl.ds(0, rows_all), :]
+    waits.append((jnp.logical_not(at_home), lambda: remote(results_gone, results_gone, ret_send.at[0], ret_recv.at[0], z, partner)))
+    some_gone = got.at[pl.ds(0, (2 * sources - 1) * capacity), :]
+    waits.append((at_home, lambda: remote(some_gone, some_gone, ret_send.at[0], ret_recv.at[0], z, partner)))
+
     odd = z % 2 == 1
     send_map = jnp.logical_and(jnp.logical_not(odd), z + 1 < nz)
     own_map = remote(map_out, map_in, m_send.at[0], m_recv.at[0], (z + 1) % nz, tp)
@@ -501,17 +537,14 @@
             across = dot(high, parts_s[1]) + dot(low, parts_s[0])
             raw = base_s[cut, :] + (dot(high, parts_s[0]) + across)
             norm = lax.rsqrt(jnp.mean(raw * raw, -1, keepdims=True) + EPSILON)
-            mo_s[cut, :] = (raw * norm * ng_s[...]).astype(BF16)
-        store_mix.start()
+            mix_out[cut, :] = (raw * norm * ng_s[...]).astype(BF16)
 
     def weights_here():
         for load in loads[8:]:
             load.wait()
         for n in range(3):
             to_partner[n].wait_recv()
-        for dt in range(1, 2 * nx):
-            sender = (tp + 2 * nx - dt) % (2 * nx)
-            remote(gains.at[sender], gains.at[sender], g_send.at[dt], g_recv.at[dt], z, sender).wait_recv()
+        gains_of_all.wait_recv()
 
     def marks(*fractions):
         found = [0]
@@ -535,16 +568,18 @@
         ready_steps(1)
         pass_map(first)
         ready_steps(nz // 4 - 1)
-        waiting = jnp.logical_and(below, c == 0)
+        waiting = jnp.logical_or(jnp.logical_and(below, c == 1), proxy)
         before, later = list(enumerate(spans[:-1]))[:2], list(enumerate(spans[:-1]))[2:]
         for n, (b, e) in before:
             gather_rows(b, e, n, True, jnp.logical_not(waiting) if n == 0 else None)
+            gather_aside(b, e, n, True)
             ready_steps(nz // 4 if n == 0 else nz // 8)
         meet_corner(spans[: len(before)])
         gather_rows(*spans[0], 0, False, waiting)
         ready_steps(nz // 8)
         for n, (b, e) in later:
             gather_rows(b, e, n)
+            gather_aside(b, e, n, False)
             ready_steps(1)
         ready_steps(nz)
         weights_here()
@@ -560,6 +595,7 @@
             make_hidden(b, e, [p for p in inner if b <= p[0] < e], n)
             if n == 0:
                 gather_rows(bulk, sources, last_span)
+                gather_aside(bulk, sources, last_span, False)
         for n in range(given, len(parts)):
             give_back(*parts[n], n)
 
@@ -577,9 +613,9 @@
         spans = marks((1, 8), (2, 8), (4, 8), (6, 8))
         count = len(spans)
 
-        def gather(n):
+        def gather(n, condition=None):
             if n < count:
-                gather_rows(*spans[n], n)
+                gather_rows(*spans[n], n, False, condition)
 
         def hide(n):
             if n < count:
@@ -591,7 +627,6 @@
 
         ready_steps(1)
         pass_map(early)
-        meet_corner()
         gather(0)
         ready_steps(2)
         gather(1)
@@ -600,12 +635,15 @@
         hide(0)
         hide(1)
         gather(2)
+        gather(3, z < nz // 2)
+        gather(4, z < nz // 2)
+        meet_corner()
         give(0)
         give(1)
         hide(2)
-        gather(3)
+        gather(3, z >= nz // 2)
         give(2)
-        gather(4)
+        gather(4, z >= nz // 2)
         for n in range(3, count):
             hide(n)
         for n in range(3, count):
@@ -618,33 +656,30 @@
     pass_map(z >= nz // 2)
     pass_state()
 
+    for condition, copy in waits:
+
+        def settle():
+            (copy() if callable(copy) else copy).wait_send()
+
+        if condition is None:
+            settle()
+        else:
+            pl.when(condition)(settle)
+
     shares = share_s[...]
     first_share = jnp.broadcast_to(shares[0:1], (tokens, tokens)).T[:, :1]
     second_share = jnp.broadcast_to(shares[1:2], (tokens, tokens)).T[:, :1]
     weights = jnp.where(slots == slot_one, first_share, 0.0) + jnp.where(slots == slot_two, second_share, 0.0)
-    for e in range(nz):
-        landing = got.at[pl.ds(e * capacity, capacity), :]
-        arrival = remote(landing, landing, disp_send.at[0], ret_recv.at[e], z, partner)
-
-        @pl.when(jnp.logical_or(e != z, parity != c))
-        def _():
-            arrival.wait_recv()
-
-    fo_s[...] = dot_left(weights, got[...]).astype(BF16)
-    store_ffn = pltpu.make_async_copy(fo_s, ffn_out, load_sem.at[14])
-    store_ffn.start()
-    for condition, copy in waits:
-
-        def settle():
-            (copy() if callable(copy) else copy).wait_send()
-
-        if condition is None:
-            settle()
-        else:
-            pl.when(condition)(settle)
-
-    store_mix.wait()
-    store_ffn.wait()
+    @pl.when(at_home)
+    def _():
+        most = got.at[pl.ds(0, (nz - 1) * capacity), :]
+        remote(most, most, ret_send.at[0], ret_recv.at[0], z, partner).wait_recv()
+
+    @pl.when(jnp.logical_not(at_home))
+    def _():
+        remote(got, got, ret_send.at[0], ret_recv.at[0], z, partner).wait_recv()
+
+    ffn_out[...] = dot_left(weights, got[...]).astype(BF16)
 
 
 def body(nz, nx, mix_query, mix_keys, mix_values, beta_in, decay_in, norm_gain, ffn_input, ffn_gain,
@@ -661,11 +696,11 @@
     call = pl.pallas_call(
         functools.partial(program_kernel, nz, nx),
         out_shape=(
-            jax.ShapeDtypeStruct((length, width), BF16),
-            jax.ShapeDtypeStruct((tokens, feats), BF16),
+            pltpu.VMEM((length, width), BF16),
+            pltpu.VMEM((tokens, feats), BF16),
         ),
         in_specs=[pl.BlockSpec(memory_space=pl.ANY)] * 13,
-        out_specs=[pl.BlockSpec(memory_space=pl.ANY)] * 2,
+        out_specs=[pl.BlockSpec(memory_space=pltpu.VMEM)] * 2,
         scratch_shapes=[
             vmem((length, width), BF16), vmem((length, width), BF16), vmem((length, width), BF16),
             vmem((1, length), F32), vmem((1, length), F32), vmem((1, width), F32),
@@ -674,18 +709,17 @@
             vmem((4 * hid, full), BF16), vmem((2, ff, feats), BF16),
             vmem((3, 8, width), F32),
             vmem((nz, capacity, feats), BF16),
-            vmem((nx, 2, rows, feats), BF16),
+            vmem((nx, 2, rows, feats), BF16), vmem((2, rows, feats), BF16),
             vmem((nx, rows, 2 * hid), BF16),
             vmem((2, rows, feats), BF16),
             vmem((2 * tokens, feats), BF16),
             vmem((length, width), F32), vmem((length, width), F32), vmem((width, 2 * width), F32),
             vmem((width, 2 * width), BF16), vmem((width, 2 * width), BF16),
             vmem((width, width), BF16), vmem((width, width), BF16), vmem((2, width, width), BF16),
-            vmem((length, width), BF16), vmem((tokens, feats), BF16),
-            dma((15,)), pltpu.SemaphoreType.REGULAR((nz,)), dma((nz,)), dma((nz // 2, 2)),
-            dma((nx, 5)), dma((nx, 5)), dma((nx, 5)), dma((nx, 5)),
-            dma((nz // 2, 2)), dma((nz,)),
-            dma((2 * nx,)), dma((2 * nx,)), dma((3,)), dma((3,)), dma((2,)), dma((1,)), dma((1,)), dma((1,)),
+            dma((13,)), pltpu.SemaphoreType.REGULAR((nz,)), dma((2,)), dma((nz // 2, 2)),
+            dma((5,)), dma((nz // 2, 2)), dma((5,)), dma((5,)), dma((5,)), dma((5,)),
+            dma((1,)), dma((1,)),
+            dma((1,)), dma((1,)), dma((3,)), dma((3,)), dma((2,)), dma((1,)), dma((1,)), dma((1,)),
         ],
         compiler_params=pltpu.CompilerParams(collective_id=0, has_side_effects=True),
     )

time: 81.9 us -> 76.1 us (0.929)
  Pallas kernels: 78.9 us -> 73.4 us
  local copies, waits for them, and re-layouts: 2.23 us -> 1.29 us
    pallas_call x1, Pallas kernels: 78.9 us -> 73.4 us  [body(): call(mix_query.reshape(length, width), mix_keys.reshape(length, width), m...]
    unnamed x4 -> x2, local copies, waits for them, and re-layouts: 2.23 us -> 1.29 us
where the time goes in v4:
time: 76.1 us; the launch traced here: 75.3 us
  Pallas kernels  73.4 us (96%)
  local copies, waits for them, and re-layouts  1.29 us (2%)
    pallas_call x1, Pallas kernels, body(): call(mix_query.reshape(length, width), mix_keys.reshape(length, width), m...  73.4 us

profile of v4, /device:TPU:80, one launch (start us, length us, event | category | flops | bytes accessed | tf_op | source)
XLA Modules:
  0.0 75.3 jit_solution(18350086858882217942)
XLA Ops:
  0.6 73.4 %shard_map.140 = (bf16[512,128]{1,0:T(8,128)(2,1)S(1)}, bf16[128,256]{1,0:T(8,128)(2,1)S(1)}) custom-call(bf16[512,128]{1,0:T(8,128)(2,1)} %bitcast.19, bf16[512,128]{1,0:T(8,128)(2,1)} %bitcast.20, bf16[512,128]{1,0:T(8,128)(2,1)} %bitcast.21, f32[1,512]{1,0:T(1,128)} %refs_3_.1, f32[1,512]{1,0:T(1,128)} %refs_4_.1, f32[1,128]{1,0:T(1,128)} %bitcast.25, ...), custom_call_target="tpu_custom_call" | custom-call | tf_op jit(solution)/shard_map/pallas_call | solution.py:726
  74.0 0.7 copy.17
  74.7 0.6 copy.18

commit v5 on v4

--- a/solution.py
+++ b/solution.py
@@ -587,16 +587,13 @@
         half = spans[min(2, last_span)][0]
         inner = [(b, e, n) for n, (b, e) in enumerate(spans)]
         parts = [(b, e) for b, e in ((0, half), (half, bulk), (bulk, sources)) if e > b]
-        given = 0
         for n, (b, e) in enumerate(parts):
-            if n == len(parts) - 1 and n > 1:
-                give_back(*parts[0], 0)
-                given = 1
             make_hidden(b, e, [p for p in inner if b <= p[0] < e], n)
             if n == 0:
                 gather_rows(bulk, sources, last_span)
                 gather_aside(bulk, sources, last_span, False)
-        for n in range(given, len(parts)):
+                give_back(*parts[0], 0)
+        for n in range(1, len(parts)):
             give_back(*parts[n], n)
 
     after = jnp.logical_not(first)
@@ -642,10 +639,11 @@
         give(1)
         hide(2)
         gather(3, z >= nz // 2)
-        give(2)
+        pl.when(z >= nz // 2)(lambda: give(2))
         gather(4, z >= nz // 2)
         for n in range(3, count):
             hide(n)
+        pl.when(z < nz // 2)(lambda: give(2))
         for n in range(3, count):
             give(n)
 

time: 76.1 us -> 75.1 us (0.987)
  no operation moved by 1% of the time
where the time goes in v5:
time: 75.1 us; the launch traced here: 74.9 us
  Pallas kernels  73 us (97%)
  local copies, waits for them, and re-layouts  1.29 us (2%)
    pallas_call x1, Pallas kernels, body(): call(mix_query.reshape(length, width), mix_keys.reshape(length, width), m...  73 us

profile of v5, /device:TPU:80, one launch (start us, length us, event | category | flops | bytes accessed | tf_op | source)
XLA Modules:
  0.0 74.9 jit_solution(5250879134189749671)
XLA Ops:
  0.6 73.0 %shard_map.140 = (bf16[512,128]{1,0:T(8,128)(2,1)S(1)}, bf16[128,256]{1,0:T(8,128)(2,1)S(1)}) custom-call(bf16[512,128]{1,0:T(8,128)(2,1)} %bitcast.19, bf16[512,128]{1,0:T(8,128)(2,1)} %bitcast.20, bf16[512,128]{1,0:T(8,128)(2,1)} %bitcast.21, f32[1,512]{1,0:T(1,128)} %refs_3_.1, f32[1,512]{1,0:T(1,128)} %refs_4_.1, f32[1,128]{1,0:T(1,128)} %bitcast.25, ...), custom_call_target="tpu_custom_call" | custom-call | tf_op jit(solution)/shard_map/pallas_call | solution.py:724
  73.6 0.7 copy.17
  74.3 0.6 copy.18
